TPU v7x, 512 devices: a whole 4x8x8 slice. The times are simulated.
512 devices in a mesh: ep: 32 (over z, x), tp: 16 (over y, core).
Axes of the slice: x: 4, y: 8, z: 8, core: 2. Of those that a mesh axis runs over, the one named last changes fastest.
Arguments:
- mixer_in: bfloat16 [4096, 2048], P('ep'), may hold values from -6 to 6
- mixer_gain: float32 [2048], replicated, may hold values from 0.1 to 1.9
- w_value: bfloat16 [2048, 1536], P(None, 'tp'), may hold values from -0.125 to 0.125
- w_gate: bfloat16 [2048, 1536], P(None, 'tp'), may hold values from -0.125 to 0.125
- w_taps: float32 [31, 1536], P(None, 'tp'), may hold values from -3 to 3
- channel_gain: float32 [1536], P('tp'), may hold values from 0.1 to 1.9
- w_output: bfloat16 [1536, 2048], P('tp'), may hold values from -0.15625 to 0.15625
- expert_in: bfloat16 [4096, 2048], P('ep'), may hold values from -6 to 6
- expert_gain: float32 [2048], replicated, may hold values from 0 to 8
- route_experts: int32 [4096, 4], P('ep'), may hold values from 0 to 31, all different within a row; in each aligned block of 128 rows (0 to 127, 128 to 255, ...) at most 32 rows name the same one
- route_scores: float32 [4096, 4], P('ep'), may hold values from -6 to 6
- expert_gate: bfloat16 [32, 2048, 2048], P('ep', None, 'tp'), may hold values from -0.125 to 0.125
- expert_up: bfloat16 [32, 2048, 2048], P('ep', None, 'tp'), may hold values from -0.125 to 0.125
- expert_down: bfloat16 [32, 2048, 2048], P('ep', 'tp'), may hold values from -0.125 to 0.125
Outputs:
- mixer_out: bfloat16 [4096, 2048], P('ep')
- expert_out: bfloat16 [4096, 2048], P('ep')
Inputs may be any that keep to these rules, and one draw needn't show every extreme that they name: `route_experts`: each row names 4 different experts. In each aligned block of 128 rows (the rows of one index of ep) no expert is named more than 32 times, a bound that some block reaches.
All inputs are finite; a program needn't handle non-finite values.
Results may differ from a plain program's by a relative error of at most 0.02.
Values may be sent and summed in bfloat16 or wider, within the bound.
No kernel may reach another device: no remote copies, remote signals or barrier semaphores. Data moves between devices by JAX's collectives and lax.ppermute only.
A program may use at most 64 MiB of HBM per device.

v0:
```python
import jax
import jax.numpy as jnp
from jax import lax
from jax.experimental import pallas as pl
from jax.experimental.pallas import tpu as pltpu
from jax.sharding import Mesh
from jax.sharding import PartitionSpec as P

CONV_CH = 1536
CONV_W = 31
TOP_K = 4
BITS = ("y2", "y1", "y0", "c")
TP = BITS
GROUP = 4
EXPERTS = 32


epsilon = 1e-05
clamp_limit = 7.0
swish_slope = 1.702


def shifted(block, axis, distance):
    devices = range(lax.axis_size(axis))
    route = [(i - distance, i) for i in devices if i - distance in devices]
    return lax.ppermute(block, axis, route)


def swapped(x, axis):
    return lax.ppermute(x, axis, [(0, 1), (1, 0)])


def exchanged(x, axis):
    return lax.all_to_all(x, axis, split_axis=0, concat_axis=0, tiled=True)


def gathered(share):
    return lax.all_gather(share, TP, axis=0, tiled=True)


def total_over(x, axis):
    size = lax.axis_size(axis)
    parts = exchanged(x.reshape(size, x.shape[0] // size, x.shape[1]), axis)
    share = jnp.sum(parts.astype(jnp.float32), axis=0).astype(jnp.bfloat16)
    return gathered(share)


def halving_total(x):
    rows, width = x.shape
    sizes = [2] * len(BITS)
    for at in reversed(range(len(BITS))):
        x = x.reshape(*sizes[: at + 1], rows // 16, width)
        own = lax.axis_index(BITS[at])
        kept = lax.dynamic_index_in_dim(x, own, at, keepdims=False)
        given = lax.dynamic_index_in_dim(x, 1 - own, at, keepdims=False)
        x = kept + swapped(given.astype(jnp.bfloat16), BITS[at]).astype(jnp.float32)
    share = x.astype(jnp.bfloat16).reshape(rows // 16, width)
    return gathered(share)


def row_norm(inputs, gains):
    widened = inputs.astype(jnp.float32)
    row_mean = jnp.mean(widened, axis=-1, keepdims=True)
    row_var = jnp.mean(jnp.square(widened - row_mean), axis=-1, keepdims=True)
    return (widened - row_mean) * lax.rsqrt(row_var + epsilon) * gains


def mixer_part(mixer_in, mixer_gain, w_value, w_gate, w_taps, channel_gain, w_output):
    normed = row_norm(mixer_in, mixer_gain).astype(jnp.bfloat16)
    values = jnp.dot(normed, w_value, preferred_element_type=jnp.float32)
    gate_pre = jnp.dot(normed, w_gate, preferred_element_type=jnp.float32)
    gated_values = (values * jax.nn.sigmoid(gate_pre)).astype(jnp.bfloat16)
    mixer_rows = gated_values.shape[0]
    reach_rows = CONV_W - 1
    earlier = shifted(gated_values[mixer_rows - reach_rows :], "ep", 1)
    extended = jnp.concatenate([earlier, gated_values], axis=0)
    conv_out = jnp.zeros(gated_values.shape, jnp.float32)
    for offset in range(CONV_W):
        conv_out = (
            conv_out + extended[offset : offset + mixer_rows].astype(jnp.float32) * w_taps[offset]
        )
    sums = jnp.stack([jnp.sum(conv_out, axis=1), jnp.sum(conv_out * conv_out, axis=1)])
    everyone = lax.all_gather(sums, TP)
    sums = jnp.sum(everyone, axis=0)
    row_mean = (sums[0] / CONV_CH)[:, None]
    row_var = (sums[1] / CONV_CH)[:, None] - row_mean * row_mean
    activated = jax.nn.silu(
        (conv_out - row_mean) * lax.rsqrt(row_var + epsilon) * channel_gain
    ).astype(jnp.bfloat16)
    return jnp.dot(activated, w_output, preferred_element_type=jnp.float32)


def front_kernel(member, x_ref, gain_ref, ids_ref, scores_ref, rows_ref, hi_ref, lo_ref):
    rows = x_ref.shape[0]
    sent = rows_ref.shape[0]
    f32, bf16 = jnp.float32, jnp.bfloat16
    normed = row_norm(x_ref[...], gain_ref[...]).astype(bf16)
    experts = EXPERTS
    slots = sent // experts
    raised = [jnp.exp(scores_ref[pl.ds(k, 1), :]) for k in range(TOP_K)]
    total = raised[0] + raised[1] + raised[2] + raised[3]
    names = lax.broadcasted_iota(jnp.int32, (experts, rows), 0)
    chosen = jnp.zeros((experts, rows), f32)
    weights = jnp.zeros((experts, rows), f32)
    for k in range(TOP_K):
        named = ids_ref[pl.ds(k, 1), :] == names
        chosen = jnp.where(named, 1.0, chosen)
        weights = jnp.where(named, raised[k] / total, weights)
    earlier = lax.broadcasted_iota(jnp.int32, (rows, rows), 0)
    later = lax.broadcasted_iota(jnp.int32, (rows, rows), 1)
    before = jnp.where(earlier < later, 1.0, 0.0).astype(bf16)
    rank = jnp.dot(chosen.astype(bf16), before, preferred_element_type=f32)
    place = jnp.where(chosen > 0.0, rank, -1.0).astype(bf16)
    of_row = lax.broadcasted_iota(jnp.int32, (sent, experts), 0) // slots
    of_col = lax.broadcasted_iota(jnp.int32, (sent, experts), 1)
    spread = jnp.where(of_row == of_col, 1.0, 0.0).astype(bf16)
    weights_hi = weights.astype(bf16)
    weights_lo = (weights - weights_hi.astype(f32)).astype(bf16)
    slot = lax.broadcasted_iota(jnp.int32, (sent, rows), 0) % slots * GROUP + member[0]
    taken = jnp.dot(spread, place, preferred_element_type=f32) == slot.astype(f32)
    select = jnp.where(taken, 1.0, 0.0).astype(bf16)
    rows_ref[...] = jnp.dot(select, normed, preferred_element_type=f32).astype(bf16)
    wide_hi = jnp.dot(spread, weights_hi, preferred_element_type=f32)
    wide_lo = jnp.dot(spread, weights_lo, preferred_element_type=f32)
    hi_ref[...] = jnp.where(taken, wide_hi, 0.0).astype(bf16)
    lo_ref[...] = jnp.where(taken, wide_lo, 0.0).astype(bf16)


def front(member, x, gain, ids, scores, sent):
    rows, width = x.shape
    whole = pl.BlockSpec(memory_space=pltpu.VMEM)
    return pl.pallas_call(
        front_kernel,
        in_specs=[pl.BlockSpec(memory_space=pltpu.SMEM)] + [whole] * 4,
        out_specs=[whole] * 3,
        out_shape=[
            jax.ShapeDtypeStruct((sent, width), jnp.bfloat16),
            jax.ShapeDtypeStruct((sent, rows), jnp.bfloat16),
            jax.ShapeDtypeStruct((sent, rows), jnp.bfloat16),
        ],
        name="front",
    )(member.reshape(1), x, gain.reshape(1, width), ids, scores)


def expert_kernel(x_ref, *refs):
    gus, downs, out_ref = refs[:GROUP], refs[GROUP : 2 * GROUP], refs[2 * GROUP]
    gu_buf, down_buf, gu_sem, down_sem = refs[2 * GROUP + 1 :]
    inner = downs[0].shape[0]
    width = out_ref.shape[1]
    gu_copies = [pltpu.make_async_copy(gus[s], gu_buf.at[s], gu_sem.at[s]) for s in range(GROUP)]
    down_copies = [
        pltpu.make_async_copy(downs[s], down_buf.at[pl.ds(s * inner, inner)], down_sem.at[s])
        for s in range(GROUP)
    ]
    for copy in gu_copies + down_copies:
        copy.start()
    hidden = []
    for s in range(GROUP):
        gu_copies[s].wait()
        both = jnp.dot(x_ref[...], gu_buf[s], preferred_element_type=jnp.float32)
        g = jnp.minimum(both[:, :inner], clamp_limit)
        u = jnp.clip(both[:, inner:], -clamp_limit, clamp_limit)
        hidden.append(((u + 1.0) * g * jax.nn.sigmoid(swish_slope * g)).astype(jnp.bfloat16))
    hidden = jnp.concatenate(hidden, axis=1)
    for copy in down_copies:
        copy.wait()
    step = 512
    for at in range(0, width, step):
        out_ref[:, at : at + step] = jnp.dot(
            hidden, down_buf[:, at : at + step], preferred_element_type=jnp.float32
        ).astype(jnp.bfloat16)


def expert(x, gus, downs):
    rows, width = x.shape
    inner = downs[0].shape[0]
    whole = pl.BlockSpec(memory_space=pltpu.VMEM)
    outside = pl.BlockSpec(memory_space=pl.ANY)
    return pl.pallas_call(
        expert_kernel,
        in_specs=[whole] + [outside] * (2 * GROUP),
        out_specs=whole,
        out_shape=jax.ShapeDtypeStruct((rows, width), jnp.bfloat16),
        scratch_shapes=[
            pltpu.VMEM((GROUP, width, 2 * inner), jnp.bfloat16),
            pltpu.VMEM((GROUP * inner, width), jnp.bfloat16),
            pltpu.SemaphoreType.DMA((GROUP,)),
            pltpu.SemaphoreType.DMA((GROUP,)),
        ],
        name="expert",
    )(x, *gus, *downs)


def program(
    mixer_in,
    mixer_gain,
    w_value,
    w_gate,
    w_taps,
    channel_gain,
    w_output,
    expert_in,
    expert_gain,
    route_experts,
    route_scores,
    expert_gate,
    expert_up,
    expert_down,
):
    rows_b, width = expert_in.shape
    experts = lax.axis_size("ep")
    capacity = 2 * rows_b * TOP_K // experts
    slots = capacity // GROUP
    member = lax.axis_index(("y0", "c")).astype(jnp.int32)

    gate_up = jnp.concatenate([expert_gate[0], expert_up[0]], axis=1)
    down = expert_down[0]
    gu_y = swapped(gate_up, "y0")
    down_y = swapped(down, "y0")
    gu_c = swapped(gate_up, "c")
    down_c = swapped(down, "c")
    gu_d = swapped(gu_y, "c")
    down_d = swapped(down_y, "c")

    sending, mixing_hi, mixing_lo = front(
        member, expert_in, expert_gain, route_experts.T, route_scores.T, experts * slots
    )
    arrived = exchanged(sending.reshape(experts, slots, width), "ep").reshape(-1, width)

    mixer_partial = mixer_part(
        mixer_in, mixer_gain, w_value, w_gate, w_taps, channel_gain, w_output
    )
    mixer_out = halving_total(mixer_partial)

    partial = expert(arrived, (gate_up, gu_c, gu_y, gu_d), (down, down_c, down_y, down_d))
    returned = exchanged(partial.reshape(experts, slots, width), "ep").reshape(-1, width)

    def mixed(m):
        return lax.dot_general(
            m, returned, (((0,), (0,)), ((), ())), preferred_element_type=jnp.float32
        )

    combined = (mixed(mixing_hi) + mixed(mixing_lo)).astype(jnp.bfloat16)
    expert_out = total_over(combined, TP)
    return (mixer_out, expert_out)


def solution(mesh):
    split = Mesh(mesh.devices.reshape(mesh.shape["ep"], 2, 2, 2, 2), ("ep", *TP))
    in_specs = (
        P("ep", None),
        P(),
        P(None, TP),
        P(None, TP),
        P(None, TP),
        P(TP),
        P(TP, None),
        P("ep", None),
        P(),
        P("ep", None),
        P("ep", None),
        P("ep", None, TP),
        P("ep", None, TP),
        P("ep", TP, None),
    )
    out_specs = (P("ep", None), P("ep", None))
    return jax.shard_map(program, mesh=split, in_specs=in_specs, out_specs=out_specs, check_vma=False)
```

profile of v0, /device:TPU:1, one launch (start us, length us, event | category | flops | bytes accessed | tf_op | source)
XLA Modules:
  0.0 186.9 jit_solution(2043707178191077373)
XLA Ops:
  0.6 0.0 copy-start
  0.6 1.4 pad_maximum_fusion.refs_0_
  2.0 4.0 %collective-permute-start.6 = (bf16[2048,256]{1,0:T(8,128)(2,1)S(1)}, bf16[2048,256]{1,0:T(8,128)(2,1)}, u32[]{:S(2)}, u32[]{:S(2)}) collective-permute-start(bf16[2048,256]{1,0:T(8,128)(2,1)S(1)} %pad_maximum_fusion.refs_0_), channel_id=1, source_target_pairs={{0,2},{2,0},{1,3},{3,1},{4,6},{6,4},{5,7},{7,5},{8,10},{10,8},{9,1... | collective-permute-start | bytes 3145736 | tf_op jit(solution)/shard_map/ppermute | solution.py:30
  6.1 6.6 %collective-permute-start.5 = (bf16[2048,256]{1,0:T(8,128)(2,1)S(1)}, bf16[2048,256]{1,0:T(8,128)(2,1)}, u32[]{:S(2)}, u32[]{:S(2)}) collective-permute-start(bf16[2048,256]{1,0:T(8,128)(2,1)S(1)} %pad_maximum_fusion.refs_0_), channel_id=1, source_target_pairs={{0,1},{1,0},{2,3},{3,2},{4,5},{5,4},{6,7},{7,6},{8,9},{9,8},{10,11... | collective-permute-start | bytes 3145736 | tf_op jit(solution)/shard_map/ppermute | solution.py:30
  12.7 3.6 %collective-permute-start.9 = (bf16[128,2048]{1,0:T(8,128)(2,1)}, bf16[128,2048]{1,0:T(8,128)(2,1)}, u32[]{:S(2)}, u32[]{:S(2)}) collective-permute-start(bf16[128,2048]{1,0:T(8,128)(2,1)} %bitcast.53.refs_4_), channel_id=1, source_target_pairs={{0,2},{2,0},{1,3},{3,1},{4,6},{6,4},{5,7},{7,5},{8,10},{10,8},{9,1... | collective-permute-start | bytes 1572872 | tf_op jit(solution)/shard_map/ppermute | solution.py:30
  16.4 2.2 %collective-permute-start.8 = (bf16[128,2048]{1,0:T(8,128)(2,1)}, bf16[128,2048]{1,0:T(8,128)(2,1)}, u32[]{:S(2)}, u32[]{:S(2)}) collective-permute-start(bf16[128,2048]{1,0:T(8,128)(2,1)} %bitcast.53.refs_4_), channel_id=1, source_target_pairs={{0,1},{1,0},{2,3},{3,2},{4,5},{5,4},{6,7},{7,6},{8,9},{9,8},{10,11... | collective-permute-start | bytes 1572872 | tf_op jit(solution)/shard_map/ppermute | solution.py:30
  18.6 2.9 %front.1 = (bf16[256,2048]{1,0:T(8,128)(2,1)}, bf16[256,128]{1,0:T(8,128)(2,1)}, bf16[256,128]{1,0:T(8,128)(2,1)}) custom-call(s32[1]{0:T(128)} %bitcast.45.member, bf16[128,2048]{1,0:T(8,128)(2,1)} %x_ref.1, f32[1,2048]{1,0:T(1,128)} %bitcast.124, s32[4,128]{1,0:T(4,128)} %bitcast.125, f32[4,128]{1,0:T(4,128)} %bitcast.126), custom_call_target="tpu_custom_call" | custom-call | tf_op jit(solution)/shard_map/front/pallas_call | solution.py:132
  21.5 7.7 %all-to-all-start = ((bf16[32,8,2048]{2,1,0:T(8,128)(2,1)}), bf16[32,8,2048]{2,1,0:T(8,128)(2,1)S(1)}, u32[]{:S(2)}, u32[]{:S(2)}) async-start(bf16[32,8,2048]{2,1,0:T(8,128)(2,1)} %bitcast.121), calls=%async_computation | async-start | bytes 2097152 | tf_op jit(solution)/shard_map/all_to_all | solution.py:34
  29.2 0.0 copy-start.11
  29.2 0.2 convert_reduce_fusion
  29.4 0.3 fusion.9
  29.7 0.5 copy-done.11
  30.2 0.4 fusion.58
  30.6 0.4 fusion.8
  31.0 0.7 slice.256
  31.7 3.7 %collective-permute-start = (bf16[30,96]{0,1:T(8,128)(2,1)}, bf16[30,96]{0,1:T(8,128)(2,1)}, u32[]{:S(2)}, u32[]{:S(2)}) collective-permute-start(bf16[30,96]{0,1:T(8,128)(2,1)} %slice.256), channel_id=1, source_target_pairs={{0,16},{16,32},{32,48},{48,64},{64,80},{80,96},{96,112},{112,128},... | collective-permute-start | bytes 17288 | tf_op jit(solution)/shard_map/ppermute | solution.py:26
  35.4 3.0 %collective-permute-start.7 = (bf16[2048,256]{1,0:T(8,128)(2,1)}, bf16[2048,256]{1,0:T(8,128)(2,1)S(1)}, u32[]{:S(2)}, u32[]{:S(2)}) collective-permute-start(bf16[2048,256]{1,0:T(8,128)(2,1)} %collective-permute-done.6.refs_2_), channel_id=1, source_target_pairs={{0,1},{1,0},{2,3},{3,2},{4,5},{5,4},{6,7},{7,6},{8,9},{9,8},{10,11... | collective-permute-start | bytes 3145736 | tf_op jit(solution)/shard_map/ppermute | solution.py:30
  38.4 0.6 slice_bitcast_fusion.30
  39.0 0.6 slice_bitcast_fusion.29
  39.7 4.4 %fusion.60 = (f32[128]{0:T(128)S(1)}, f32[128]{0:T(128)S(1)}, f32[128,96]{0,1:T(8,128)}) fusion(f32[96]{0:T(128)} %get-tuple-element.40, bf16[128,96]{0,1:T(8,128)(2,1)} %copy-done.6, f32[96]{0:T(128)} %get-tuple-element.41, bf16[30,96]{0,1:T(8,128)(2,1)} %collective-permute-done, f32[96]{0:T(128)S(1)} %get-tuple-element.12, f32[96]{0:T(128)S(1)} %get-tuple-element.13, ...), kind=kLoop, calls=%fused_computation.171 | loop fusion | flops 2273024 | bytes 92416 | tf_op jit(solution)/shard_map/reduce_sum | solution.py:82
  44.1 1.9 %collective-permute-start.10 = (bf16[128,2048]{1,0:T(8,128)(2,1)}, bf16[128,2048]{1,0:T(8,128)(2,1)}, u32[]{:S(2)}, u32[]{:S(2)}) collective-permute-start(bf16[128,2048]{1,0:T(8,128)(2,1)} %collective-permute-done.9.refs_6_), channel_id=1, source_target_pairs={{0,1},{1,0},{2,3},{3,2},{4,5},{5,4},{6,7},{7,6},{8,9},{9,8},{10,11... | collective-permute-start | bytes 1572872 | tf_op jit(solution)/shard_map/ppermute | solution.py:30
  46.1 18.0 %all-gather.1 = f32[16,2,128]{2,1,0:T(2,128)S(1)} all-gather(f32[1,2,128]{2,1,0:T(2,128)S(1)} %maximum_bitcast_fusion), channel_id=2, replica_groups=mesh['ep'=32,'y2'=2,'y1'=2,'y0'=2,'c'=2] {'y2','y1','y0','c'}, dimensions={0}, use_global_device_ids=true | all-gather | bytes 17408 | tf_op jit(solution)/shard_map/all_gather | solution.py:83
  64.0 0.6 reduce_sum.61
  64.6 0.7 fusion.55
  65.3 0.6 multiply_bitcast_fusion
  66.0 0.9 copy-done.2
  67.0 0.4 copy-done.4
  67.3 7.0 %expert.1 = bf16[256,2048]{1,0:T(8,128)(2,1)} custom-call(bf16[256,2048]{1,0:T(8,128)(2,1)} %bitcast.117, bf16[2048,256]{1,0:T(8,128)(2,1)} %copy-done.1, bf16[2048,256]{1,0:T(8,128)(2,1)} %collective-permute-done.5.refs_1_, bf16[2048,256]{1,0:T(8,128)(2,1)} %collective-permute-done.6.refs_2_, bf16[2048,256]{1,0:T(8,128)(2,1)} %copy-done.4, ...), custom_call_target="tpu_custom_call" | custom-call | tf_op jit(solution)/shard_map/expert/pallas_call | solution.py:179
  74.4 0.0 copy-start.10
  74.4 23.1 %all-to-all-start.1 = ((bf16[32,8,2048]{2,1,0:T(8,128)(2,1)}), bf16[32,8,2048]{2,1,0:T(8,128)(2,1)S(1)}, u32[]{:S(2)}, u32[]{:S(2)}) async-start(bf16[32,8,2048]{2,1,0:T(8,128)(2,1)} %bitcast.118), calls=%async_computation.1 | async-start | bytes 2097152 | tf_op jit(solution)/shard_map/all_to_all | solution.py:34
  97.6 0.4 fusion.20
  98.0 2.4 %collective-permute-start.1 = (bf16[2,2,2,8,2048]{4,3,0,1,2:T(8,128)(2,1)S(1)}, bf16[2,2,2,8,2048]{4,3,0,1,2:T(8,128)(2,1)S(1)}, u32[]{:S(2)}, u32[]{:S(2)}) collective-permute-start(bf16[2,2,2,8,2048]{4,3,0,1,2:T(8,128)(2,1)S(1)} %fusion.15), channel_id=1, source_target_pairs={{0,1},{1,0},{2,3},{3,2},{4,5},{5,4},{6,7},{7,6},{8,9},{9,8},{10,11... | collective-permute-start | bytes 786440 | tf_op jit(solution)/shard_map/ppermute | solution.py:30
  100.4 1.1 collective-permute-done.1
  101.6 1.9 %collective-permute-start.2 = (bf16[2,2,8,2048]{3,2,0,1:T(8,128)(2,1)S(1)}, bf16[2,2,8,2048]{3,2,0,1:T(8,128)(2,1)S(1)}, u32[]{:S(2)}, u32[]{:S(2)}) collective-permute-start(bf16[2,2,8,2048]{3,2,0,1:T(8,128)(2,1)S(1)} %fusion.16), channel_id=1, source_target_pairs={{0,2},{2,0},{1,3},{3,1},{4,6},{6,4},{5,7},{7,5},{8,10},{10,8},{9,1... | collective-permute-start | bytes 393224 | tf_op jit(solution)/shard_map/ppermute | solution.py:30
  103.5 4.6 %collective-permute-done.2 = bf16[2,2,8,2048]{3,2,0,1:T(8,128)(2,1)S(1)} collective-permute-done((bf16[2,2,8,2048]{3,2,0,1:T(8,128)(2,1)S(1)}, bf16[2,2,8,2048]{3,2,0,1:T(8,128)(2,1)S(1)}, u32[]{:S(2)}, u32[]{:S(2)}) %collective-permute-start.2) | collective-permute-done | bytes 131104 | tf_op jit(solution)/shard_map/ppermute | solution.py:30
  108.2 2.5 %collective-permute-start.3 = (bf16[2,8,2048]{2,1,0:T(8,128)(2,1)S(1)}, bf16[2,8,2048]{2,1,0:T(8,128)(2,1)S(1)}, u32[]{:S(2)}, u32[]{:S(2)}) collective-permute-start(bf16[2,8,2048]{2,1,0:T(8,128)(2,1)S(1)} %fusion.17), channel_id=1, source_target_pairs={{0,4},{4,0},{1,5},{5,1},{2,6},{6,2},{3,7},{7,3},{8,12},{12,8},{9,1... | collective-permute-start | bytes 196616 | tf_op jit(solution)/shard_map/ppermute | solution.py:30
  110.7 13.9 %all-to-all-done.1 = bf16[32,8,2048]{2,1,0:T(8,128)(2,1)S(1)} async-done(((bf16[32,8,2048]{2,1,0:T(8,128)(2,1)}), bf16[32,8,2048]{2,1,0:T(8,128)(2,1)S(1)}, u32[]{:S(2)}, u32[]{:S(2)}) %all-to-all-start.1) | async-done | bytes 1048608 | tf_op jit(solution)/shard_map/all_to_all | solution.py:34
  124.6 0.3 fusion.12
  124.9 0.5 copy-done.8
  125.5 1.1 fusion.1
  126.6 6.2 %all-to-all-start.2 = ((bf16[16,8,2048]{2,1,0:T(8,128)(2,1)}), bf16[16,8,2048]{2,1,0:T(8,128)(2,1)S(1)}, u32[]{:S(2)}, u32[]{:S(2)}) async-start(bf16[16,8,2048]{2,1,0:T(8,128)(2,1)} %fusion.1), calls=%async_computation.2 | async-start | bytes 1048576 | tf_op jit(solution)/shard_map/all_to_all | solution.py:34
  132.9 7.2 %collective-permute-start.4 = (bf16[8,2048]{1,0:T(8,128)(2,1)S(1)}, bf16[8,2048]{1,0:T(8,128)(2,1)S(1)}, u32[]{:S(2)}, u32[]{:S(2)}) collective-permute-start(bf16[8,2048]{1,0:T(8,128)(2,1)S(1)} %fusion.19), channel_id=1, source_target_pairs={{0,8},{8,0},{1,9},{9,1},{2,10},{10,2},{3,11},{11,3},{4,12},{12,4},... | collective-permute-start | bytes 98312 | tf_op jit(solution)/shard_map/ppermute | solution.py:30
  140.1 10.5 %collective-permute-done.4 = bf16[8,2048]{1,0:T(8,128)(2,1)S(1)} collective-permute-done((bf16[8,2048]{1,0:T(8,128)(2,1)S(1)}, bf16[8,2048]{1,0:T(8,128)(2,1)S(1)}, u32[]{:S(2)}, u32[]{:S(2)}) %collective-permute-start.4) | collective-permute-done | bytes 32800 | tf_op jit(solution)/shard_map/ppermute | solution.py:30
  150.6 18.0 %all_gather.14 = bf16[128,2048]{1,0:T(8,128)(2,1)S(1)} all-gather(bf16[8,2048]{1,0:T(8,128)(2,1)S(1)} %fusion.18), channel_id=1, replica_groups=mesh['ep'=32,'y2'=2,'y1'=2,'y0'=2,'c'=2] {'y2','y1','y0','c'}, dimensions={0}, use_global_device_ids=true | all-gather | bytes 557056 | tf_op jit(solution)/shard_map/all_gather | solution.py:38
  168.5 0.1 reduce_sum.62
  168.6 16.7 %all_gather.15 = bf16[128,2048]{1,0:T(8,128)(2,1)S(1)} all-gather(bf16[8,2048]{1,0:T(8,128)(2,1)S(1)} %reduce_sum.62), channel_id=1, replica_groups=mesh['ep'=32,'y2'=2,'y1'=2,'y0'=2,'c'=2] {'y2','y1','y0','c'}, dimensions={0}, use_global_device_ids=true | all-gather | bytes 557056 | tf_op jit(solution)/shard_map/all_gather | solution.py:38
  185.3 0.8 copy.27
  186.1 0.8 copy.28
  (42 shorter events, 0.3 us)
Async XLA Ops:
  0.6 96.9 %copy-start = (bf16[96,2048]{1,0:T(8,128)(2,1)S(1)}, bf16[96,2048]{1,0:T(8,128)(2,1)}, u32[]{:S(2)}) copy-start(bf16[96,2048]{1,0:T(8,128)(2,1)} %param.20) | copy-start | bytes 1179652
  2.0 19.5 %copy-start.1 = (bf16[2048,256]{1,0:T(8,128)(2,1)}, bf16[2048,256]{1,0:T(8,128)(2,1)S(1)}, u32[]{:S(2)}) copy-start(bf16[2048,256]{1,0:T(8,128)(2,1)S(1)} %pad_maximum_fusion.refs_0_) | copy-start | bytes 3145732
  2.0 33.4 %collective-permute-start.6 = (bf16[2048,256]{1,0:T(8,128)(2,1)S(1)}, bf16[2048,256]{1,0:T(8,128)(2,1)}, u32[]{:S(2)}, u32[]{:S(2)}) collective-permute-start(bf16[2048,256]{1,0:T(8,128)(2,1)S(1)} %pad_maximum_fusion.refs_0_), channel_id=1, source_target_pairs={{0,2},{2,0},{1,3},{3,1},{4,6},{6,4},{5,7},{7,5},{8,10},{10,8},{9,1... | collective-permute-start | bytes 3145736 | tf_op jit(solution)/shard_map/ppermute | solution.py:30
  6.1 59.9 %collective-permute-start.5 = (bf16[2048,256]{1,0:T(8,128)(2,1)S(1)}, bf16[2048,256]{1,0:T(8,128)(2,1)}, u32[]{:S(2)}, u32[]{:S(2)}) collective-permute-start(bf16[2048,256]{1,0:T(8,128)(2,1)S(1)} %pad_maximum_fusion.refs_0_), channel_id=1, source_target_pairs={{0,1},{1,0},{2,3},{3,2},{4,5},{5,4},{6,7},{7,6},{8,9},{9,8},{10,11... | collective-permute-start | bytes 3145736 | tf_op jit(solution)/shard_map/ppermute | solution.py:30
  12.7 31.4 %collective-permute-start.9 = (bf16[128,2048]{1,0:T(8,128)(2,1)}, bf16[128,2048]{1,0:T(8,128)(2,1)}, u32[]{:S(2)}, u32[]{:S(2)}) collective-permute-start(bf16[128,2048]{1,0:T(8,128)(2,1)} %bitcast.53.refs_4_), channel_id=1, source_target_pairs={{0,2},{2,0},{1,3},{3,1},{4,6},{6,4},{5,7},{7,5},{8,10},{10,8},{9,1... | collective-permute-start | bytes 1572872 | tf_op jit(solution)/shard_map/ppermute | solution.py:30
  16.4 49.6 %collective-permute-start.8 = (bf16[128,2048]{1,0:T(8,128)(2,1)}, bf16[128,2048]{1,0:T(8,128)(2,1)}, u32[]{:S(2)}, u32[]{:S(2)}) collective-permute-start(bf16[128,2048]{1,0:T(8,128)(2,1)} %bitcast.53.refs_4_), channel_id=1, source_target_pairs={{0,1},{1,0},{2,3},{3,2},{4,5},{5,4},{6,7},{7,6},{8,9},{9,8},{10,11... | collective-permute-start | bytes 1572872 | tf_op jit(solution)/shard_map/ppermute | solution.py:30
  21.5 7.7 %copy-start.3 = (bf16[128,2048]{1,0:T(8,128)(2,1)S(1)}, bf16[128,2048]{1,0:T(8,128)(2,1)}, u32[]{:S(2)}) copy-start(bf16[128,2048]{1,0:T(8,128)(2,1)} %param.14) | copy-start | bytes 1572868
  21.5 44.5 %all-to-all-start = ((bf16[32,8,2048]{2,1,0:T(8,128)(2,1)}), bf16[32,8,2048]{2,1,0:T(8,128)(2,1)S(1)}, u32[]{:S(2)}, u32[]{:S(2)}) async-start(bf16[32,8,2048]{2,1,0:T(8,128)(2,1)} %bitcast.121), calls=%async_computation | async-start | bytes 2097152 | tf_op jit(solution)/shard_map/all_to_all | solution.py:34
  29.2 1.0 copy-start.11
  29.2 1.0 copy-start.13
  29.4 1.2 copy-start.12
  30.6 7.8 %copy-start.9 = (f32[31,96]{1,0:T(8,128)S(1)}, f32[31,96]{1,0:T(8,128)}, u32[]{:S(2)}) copy-start(f32[31,96]{1,0:T(8,128)} %param.18) | copy-start | bytes 35716
  31.0 4.4 %copy-start.6 = (bf16[128,96]{0,1:T(8,128)(2,1)}, bf16[128,96]{0,1:T(8,128)(2,1)S(1)}, u32[]{:S(2)}) copy-start(bf16[128,96]{0,1:T(8,128)(2,1)S(1)} %fusion.8) | copy-start | bytes 73732
  31.7 8.0 %collective-permute-start = (bf16[30,96]{0,1:T(8,128)(2,1)}, bf16[30,96]{0,1:T(8,128)(2,1)}, u32[]{:S(2)}, u32[]{:S(2)}) collective-permute-start(bf16[30,96]{0,1:T(8,128)(2,1)} %slice.256), channel_id=1, source_target_pairs={{0,16},{16,32},{32,48},{48,64},{64,80},{80,96},{96,112},{112,128},... | collective-permute-start | bytes 17288 | tf_op jit(solution)/shard_map/ppermute | solution.py:26
  35.4 30.6 %collective-permute-start.7 = (bf16[2048,256]{1,0:T(8,128)(2,1)}, bf16[2048,256]{1,0:T(8,128)(2,1)S(1)}, u32[]{:S(2)}, u32[]{:S(2)}) collective-permute-start(bf16[2048,256]{1,0:T(8,128)(2,1)} %collective-permute-done.6.refs_2_), channel_id=1, source_target_pairs={{0,1},{1,0},{2,3},{3,2},{4,5},{5,4},{6,7},{7,6},{8,9},{9,8},{10,11... | collective-permute-start | bytes 3145736 | tf_op jit(solution)/shard_map/ppermute | solution.py:30
  44.1 21.8 %collective-permute-start.10 = (bf16[128,2048]{1,0:T(8,128)(2,1)}, bf16[128,2048]{1,0:T(8,128)(2,1)}, u32[]{:S(2)}, u32[]{:S(2)}) collective-permute-start(bf16[128,2048]{1,0:T(8,128)(2,1)} %collective-permute-done.9.refs_6_), channel_id=1, source_target_pairs={{0,1},{1,0},{2,3},{3,2},{4,5},{5,4},{6,7},{7,6},{8,9},{9,8},{10,11... | collective-permute-start | bytes 1572872 | tf_op jit(solution)/shard_map/ppermute | solution.py:30
  66.0 1.0 copy-start.2
  66.0 1.3 copy-start.4
  74.4 23.1 %copy-start.5 = (f32[128,96]{0,1:T(8,128)S(1)}, f32[128,96]{0,1:T(8,128)}, u32[]{:S(2)}) copy-start(f32[128,96]{0,1:T(8,128)} %get-tuple-element.10) | copy-start | bytes 147460
  74.4 23.1 %copy-start.10 = (f32[96]{0:T(128)S(1)}, f32[96]{0:T(128)}, u32[]{:S(2)}) copy-start(f32[96]{0:T(128)} %param.19) | copy-start | bytes 1156
  74.4 50.2 %all-to-all-start.1 = ((bf16[32,8,2048]{2,1,0:T(8,128)(2,1)}), bf16[32,8,2048]{2,1,0:T(8,128)(2,1)S(1)}, u32[]{:S(2)}, u32[]{:S(2)}) async-start(bf16[32,8,2048]{2,1,0:T(8,128)(2,1)} %bitcast.118), calls=%async_computation.1 | async-start | bytes 2097152 | tf_op jit(solution)/shard_map/all_to_all | solution.py:34
  98.0 3.5 %collective-permute-start.1 = (bf16[2,2,2,8,2048]{4,3,0,1,2:T(8,128)(2,1)S(1)}, bf16[2,2,2,8,2048]{4,3,0,1,2:T(8,128)(2,1)S(1)}, u32[]{:S(2)}, u32[]{:S(2)}) collective-permute-start(bf16[2,2,2,8,2048]{4,3,0,1,2:T(8,128)(2,1)S(1)} %fusion.15), channel_id=1, source_target_pairs={{0,1},{1,0},{2,3},{3,2},{4,5},{5,4},{6,7},{7,6},{8,9},{9,8},{10,11... | collective-permute-start | bytes 786440 | tf_op jit(solution)/shard_map/ppermute | solution.py:30
  100.4 24.2 %copy-start.7 = (bf16[256,128]{1,0:T(8,128)(2,1)S(1)}, bf16[256,128]{1,0:T(8,128)(2,1)}, u32[]{:S(2)}) copy-start(bf16[256,128]{1,0:T(8,128)(2,1)} %get-tuple-element.7) | copy-start | bytes 196612
  101.6 6.6 %collective-permute-start.2 = (bf16[2,2,8,2048]{3,2,0,1:T(8,128)(2,1)S(1)}, bf16[2,2,8,2048]{3,2,0,1:T(8,128)(2,1)S(1)}, u32[]{:S(2)}, u32[]{:S(2)}) collective-permute-start(bf16[2,2,8,2048]{3,2,0,1:T(8,128)(2,1)S(1)} %fusion.16), channel_id=1, source_target_pairs={{0,2},{2,0},{1,3},{3,1},{4,6},{6,4},{5,7},{7,5},{8,10},{10,8},{9,1... | collective-permute-start | bytes 393224 | tf_op jit(solution)/shard_map/ppermute | solution.py:30
  108.2 24.6 %collective-permute-start.3 = (bf16[2,8,2048]{2,1,0:T(8,128)(2,1)S(1)}, bf16[2,8,2048]{2,1,0:T(8,128)(2,1)S(1)}, u32[]{:S(2)}, u32[]{:S(2)}) collective-permute-start(bf16[2,8,2048]{2,1,0:T(8,128)(2,1)S(1)} %fusion.17), channel_id=1, source_target_pairs={{0,4},{4,0},{1,5},{5,1},{2,6},{6,2},{3,7},{7,3},{8,12},{12,8},{9,1... | collective-permute-start | bytes 196616 | tf_op jit(solution)/shard_map/ppermute | solution.py:30
  124.6 0.8 copy-start.8
  126.6 42.0 %all-to-all-start.2 = ((bf16[16,8,2048]{2,1,0:T(8,128)(2,1)}), bf16[16,8,2048]{2,1,0:T(8,128)(2,1)S(1)}, u32[]{:S(2)}, u32[]{:S(2)}) async-start(bf16[16,8,2048]{2,1,0:T(8,128)(2,1)} %fusion.1), calls=%async_computation.2 | async-start | bytes 1048576 | tf_op jit(solution)/shard_map/all_to_all | solution.py:34
  132.9 17.7 %collective-permute-start.4 = (bf16[8,2048]{1,0:T(8,128)(2,1)S(1)}, bf16[8,2048]{1,0:T(8,128)(2,1)S(1)}, u32[]{:S(2)}, u32[]{:S(2)}) collective-permute-start(bf16[8,2048]{1,0:T(8,128)(2,1)S(1)} %fusion.19), channel_id=1, source_target_pairs={{0,8},{8,0},{1,9},{9,1},{2,10},{10,2},{3,11},{11,3},{4,12},{12,4},... | collective-permute-start | bytes 98312 | tf_op jit(solution)/shard_map/ppermute | solution.py:30
where the time goes:
time: 188 us; the launch traced here: 187 us
  starting transfers between devices  76 us (40%)
  blocking collectives  52.6 us (28%)
  waiting for transfers between devices  30.2 us (16%)
  Pallas kernels  9.93 us (5%)
  other arithmetic  8.38 us (4%)
  local copies, waits for them, and re-layouts  6.03 us (3%)
  matrix products  2.68 us (1%)
    all_to_all x3, starting transfers between devices, exchanged(): return lax.all_to_all(x, axis, split_axis=0, concat_axis=0, tiled=True)  37 us
    ppermute x10, starting transfers between devices, swapped(): return lax.ppermute(x, axis, [(0, 1), (1, 0)])  35.3 us
    all_gather x2, blocking collectives, gathered(): return lax.all_gather(share, TP, axis=0, tiled=True)  34.6 us
    all_gather x1, blocking collectives, mixer_part(): everyone = lax.all_gather(sums, TP)  18 us
    ppermute x10, waiting for transfers between devices, swapped(): return lax.ppermute(x, axis, [(0, 1), (1, 0)])  16.3 us
    all_to_all x3, waiting for transfers between devices, exchanged(): return lax.all_to_all(x, axis, split_axis=0, concat_axis=0, tiled=True)  13.9 us
    pallas_call x1, Pallas kernels, expert(): pl.pallas_call(expert_kernel, in_specs=[whole] + [outside] * (2 * GROUP),...  7.05 us
    reduce_sum x1, other arithmetic, mixer_part(): jnp.sum(conv_out, axis=1)  4.44 us
  transfers between devices with their start and end apart: 14, of which 4 were waited for; matrix products, arithmetic and copies ran while one was open for 6% of the time, Pallas kernels for 2%

commit v1 on v0

--- a/solution.py
+++ b/solution.py
@@ -80,7 +80,8 @@
             conv_out + extended[offset : offset + mixer_rows].astype(jnp.float32) * w_taps[offset]
         )
     sums = jnp.stack([jnp.sum(conv_out, axis=1), jnp.sum(conv_out * conv_out, axis=1)])
-    everyone = lax.all_gather(sums, TP)
+    copies = jnp.broadcast_to(sums, (lax.axis_size(TP), *sums.shape))
+    everyone = exchanged(copies, TP)
     sums = jnp.sum(everyone, axis=0)
     row_mean = (sums[0] / CONV_CH)[:, None]
     row_var = (sums[1] / CONV_CH)[:, None] - row_mean * row_mean
@@ -142,50 +143,68 @@
     )(member.reshape(1), x, gain.reshape(1, width), ids, scores)
 
 
-def expert_kernel(x_ref, *refs):
-    gus, downs, out_ref = refs[:GROUP], refs[GROUP : 2 * GROUP], refs[2 * GROUP]
-    gu_buf, down_buf, gu_sem, down_sem = refs[2 * GROUP + 1 :]
+def expert_kernel(x_hbm, *refs):
+    gus, downs, out_hbm = refs[:GROUP], refs[GROUP : 2 * GROUP], refs[2 * GROUP]
+    x_buf, gu_buf, down_buf, out_buf, x_sem, gu_sem, down_sem, out_sem = refs[2 * GROUP + 1 :]
     inner = downs[0].shape[0]
-    width = out_ref.shape[1]
+    width = out_hbm.shape[1]
+    x_copy = pltpu.make_async_copy(x_hbm, x_buf, x_sem)
     gu_copies = [pltpu.make_async_copy(gus[s], gu_buf.at[s], gu_sem.at[s]) for s in range(GROUP)]
     down_copies = [
         pltpu.make_async_copy(downs[s], down_buf.at[pl.ds(s * inner, inner)], down_sem.at[s])
         for s in range(GROUP)
     ]
-    for copy in gu_copies + down_copies:
-        copy.start()
+    x_copy.start()
+    gu_copies[0].start()
+    gu_copies[1].start()
+    x_copy.wait()
     hidden = []
     for s in range(GROUP):
         gu_copies[s].wait()
-        both = jnp.dot(x_ref[...], gu_buf[s], preferred_element_type=jnp.float32)
+        if s + 2 < GROUP:
+            gu_copies[s + 2].start()
+        down_copies[s].start()
+        both = jnp.dot(x_buf[...], gu_buf[s], preferred_element_type=jnp.float32)
         g = jnp.minimum(both[:, :inner], clamp_limit)
         u = jnp.clip(both[:, inner:], -clamp_limit, clamp_limit)
         hidden.append(((u + 1.0) * g * jax.nn.sigmoid(swish_slope * g)).astype(jnp.bfloat16))
     hidden = jnp.concatenate(hidden, axis=1)
     for copy in down_copies:
         copy.wait()
-    step = 512
-    for at in range(0, width, step):
-        out_ref[:, at : at + step] = jnp.dot(
-            hidden, down_buf[:, at : at + step], preferred_element_type=jnp.float32
+    parts = out_sem.shape[0]
+    step = width // parts
+    out_copies = []
+    for n in range(parts):
+        own = pl.ds(n * step, step)
+        out_buf[:, own] = jnp.dot(
+            hidden, down_buf[:, own], preferred_element_type=jnp.float32
         ).astype(jnp.bfloat16)
+        copy = pltpu.make_async_copy(out_buf.at[:, own], out_hbm.at[:, own], out_sem.at[n])
+        copy.start()
+        out_copies.append(copy)
+    for copy in out_copies:
+        copy.wait()
 
 
 def expert(x, gus, downs):
     rows, width = x.shape
     inner = downs[0].shape[0]
-    whole = pl.BlockSpec(memory_space=pltpu.VMEM)
+    parts = 4
     outside = pl.BlockSpec(memory_space=pl.ANY)
     return pl.pallas_call(
         expert_kernel,
-        in_specs=[whole] + [outside] * (2 * GROUP),
-        out_specs=whole,
+        in_specs=[outside] * (1 + 2 * GROUP),
+        out_specs=outside,
         out_shape=jax.ShapeDtypeStruct((rows, width), jnp.bfloat16),
         scratch_shapes=[
+            pltpu.VMEM((rows, width), jnp.bfloat16),
             pltpu.VMEM((GROUP, width, 2 * inner), jnp.bfloat16),
             pltpu.VMEM((GROUP * inner, width), jnp.bfloat16),
+            pltpu.VMEM((rows, width), jnp.bfloat16),
+            pltpu.SemaphoreType.DMA,
             pltpu.SemaphoreType.DMA((GROUP,)),
             pltpu.SemaphoreType.DMA((GROUP,)),
+            pltpu.SemaphoreType.DMA((parts,)),
         ],
         name="expert",
     )(x, *gus, *downs)

time: 188 us -> 183 us (0.973)
  waiting for transfers between devices: 30.2 us -> 51.9 us
  blocking collectives: 52.6 us -> 34.4 us
  starting transfers between devices: 76 us -> 70.9 us
  local copies, waits for them, and re-layouts: 6.03 us -> 3.96 us
    all_gather x1 -> x0, blocking collectives: 18 us -> none  [mixer_part(): everyone = lax.all_gather(sums, TP)]
    all_to_all x3 -> x4, waiting for transfers between devices: 13.9 us -> 31.2 us  [exchanged(): return lax.all_to_all(x, axis, split_axis=0, concat_axis=0, tiled=True)]
    ppermute x10, waiting for transfers between devices: 16.3 us -> 20.7 us  [swapped(): return lax.ppermute(x, axis, [(0, 1), (1, 0)])]
    all_to_all x3 -> x4, starting transfers between devices: 37 us -> 33.2 us  [exchanged(): return lax.all_to_all(x, axis, split_axis=0, concat_axis=0, tiled=True)]
    reduce_sum x1, other arithmetic: 4.44 us -> 1.51 us  [mixer_part(): jnp.sum(conv_out, axis=1)]
    unnamed x30 -> x36, local copies, waits for them, and re-layouts: 3.98 us -> 3.16 us
  transfers between devices with their start and end apart: 14 -> 15, of which waited for: 4 -> 7; matrix products, arithmetic and copies ran while one was open for 6% -> 4% of each run, Pallas kernels for 2% -> 2%
where the time goes in v1:
time: 183 us; the launch traced here: 182 us
  starting transfers between devices  70.9 us (39%)
  waiting for transfers between devices  51.9 us (28%)
  blocking collectives  34.4 us (19%)
  Pallas kernels  9.16 us (5%)
  other arithmetic  7.53 us (4%)
  local copies, waits for them, and re-layouts  3.96 us (2%)
  matrix products  2.68 us (1%)
    all_gather x2, blocking collectives, gathered(): return lax.all_gather(share, TP, axis=0, tiled=True)  34.4 us
    ppermute x10, starting transfers between devices, swapped(): return lax.ppermute(x, axis, [(0, 1), (1, 0)])  33.8 us
    all_to_all x4, starting transfers between devices, exchanged(): return lax.all_to_all(x, axis, split_axis=0, concat_axis=0, tiled=True)  33.2 us
    all_to_all x4, waiting for transfers between devices, exchanged(): return lax.all_to_all(x, axis, split_axis=0, concat_axis=0, tiled=True)  31.2 us
    ppermute x10, waiting for transfers between devices, swapped(): return lax.ppermute(x, axis, [(0, 1), (1, 0)])  20.7 us
    pallas_call x1, Pallas kernels, expert(): pl.pallas_call(expert_kernel, in_specs=[outside] * (1 + 2 * GROUP), out_s...  6.3 us
    ppermute x1, starting transfers between devices, shifted(): return lax.ppermute(block, axis, route)  3.93 us
  transfers between devices with their start and end apart: 15, of which 7 were waited for; matrix products, arithmetic and copies ran while one was open for 4% of the time, Pallas kernels for 2%

profile of v1, /device:TPU:1, one launch (start us, length us, event | category | flops | bytes accessed | tf_op | source)
XLA Modules:
  0.0 181.7 jit_solution(1151114515852853387)
XLA Ops:
  0.6 0.0 copy-start
  0.6 0.0 copy-start.3
  0.7 1.3 convert_reduce_fusion
  2.0 1.4 fusion.9
  3.4 0.4 fusion.58
  3.8 0.0 copy-start.5
  3.8 0.4 fusion.8
  4.3 0.1 slice.256
  4.3 3.9 %collective-permute-start = (bf16[30,96]{0,1:T(8,128)(2,1)S(1)}, bf16[30,96]{0,1:T(8,128)(2,1)S(1)}, u32[]{:S(2)}, u32[]{:S(2)}) collective-permute-start(bf16[30,96]{0,1:T(8,128)(2,1)S(1)} %slice.256), channel_id=1, source_target_pairs={{0,16},{16,32},{32,48},{48,64},{64,80},{80,96},{96,112},{112,128},... | collective-permute-start | bytes 17288 | tf_op jit(solution)/shard_map/ppermute | solution.py:26
  8.3 0.1 pad_maximum_fusion.refs_0_
  8.4 3.2 %collective-permute-start.6 = (bf16[2048,256]{1,0:T(8,128)(2,1)S(1)}, bf16[2048,256]{1,0:T(8,128)(2,1)S(1)}, u32[]{:S(2)}, u32[]{:S(2)}) collective-permute-start(bf16[2048,256]{1,0:T(8,128)(2,1)S(1)} %pad_maximum_fusion.refs_0_), channel_id=1, source_target_pairs={{0,2},{2,0},{1,3},{3,1},{4,6},{6,4},{5,7},{7,5},{8,10},{10,8},{9,1... | collective-permute-start | bytes 3145736 | tf_op jit(solution)/shard_map/ppermute | solution.py:30
  11.7 1.5 fusion.60
  13.2 0.6 broadcast_in_dim.2
  13.8 7.4 %all-to-all-start = ((f32[16,2,128]{2,1,0:T(2,128)}), f32[16,2,128]{2,1,0:T(2,128)S(1)}, u32[]{:S(2)}, u32[]{:S(2)}) async-start(f32[16,2,128]{2,1,0:T(2,128)} %broadcast_in_dim.2), calls=%async_computation | async-start | bytes 32768 | tf_op jit(solution)/shard_map/all_to_all | solution.py:34
  21.3 2.9 %front.1 = (bf16[256,2048]{1,0:T(8,128)(2,1)}, bf16[256,128]{1,0:T(8,128)(2,1)}, bf16[256,128]{1,0:T(8,128)(2,1)}) custom-call(s32[1]{0:T(128)} %bitcast.44.member, bf16[128,2048]{1,0:T(8,128)(2,1)} %x_ref.1, f32[1,2048]{1,0:T(1,128)} %bitcast.125, s32[4,128]{1,0:T(4,128)} %bitcast.126, f32[4,128]{1,0:T(4,128)} %bitcast.127), custom_call_target="tpu_custom_call" | custom-call | tf_op jit(solution)/shard_map/front/pallas_call | solution.py:133
  24.2 16.1 %all-to-all-done = f32[16,2,128]{2,1,0:T(2,128)S(1)} async-done(((f32[16,2,128]{2,1,0:T(2,128)}), f32[16,2,128]{2,1,0:T(2,128)S(1)}, u32[]{:S(2)}, u32[]{:S(2)}) %all-to-all-start) | async-done | bytes 16416 | tf_op jit(solution)/shard_map/all_to_all | solution.py:34
  40.2 12.6 %all-to-all-start.1 = ((bf16[32,8,2048]{2,1,0:T(8,128)(2,1)}), bf16[32,8,2048]{2,1,0:T(8,128)(2,1)S(1)}, u32[]{:S(2)}, u32[]{:S(2)}) async-start(bf16[32,8,2048]{2,1,0:T(8,128)(2,1)} %bitcast.119), calls=%async_computation.1 | async-start | bytes 2097152 | tf_op jit(solution)/shard_map/all_to_all | solution.py:34
  52.8 3.0 %collective-permute-start.9 = (bf16[128,2048]{1,0:T(8,128)(2,1)}, bf16[128,2048]{1,0:T(8,128)(2,1)}, u32[]{:S(2)}, u32[]{:S(2)}) collective-permute-start(bf16[128,2048]{1,0:T(8,128)(2,1)} %bitcast.120), channel_id=1, source_target_pairs={{0,2},{2,0},{1,3},{3,1},{4,6},{6,4},{5,7},{7,5},{8,10},{10,8},{9,1... | collective-permute-start | bytes 1572872 | tf_op jit(solution)/shard_map/ppermute | solution.py:30
  55.8 2.9 %collective-permute-start.5 = (bf16[2048,256]{1,0:T(8,128)(2,1)S(1)}, bf16[2048,256]{1,0:T(8,128)(2,1)}, u32[]{:S(2)}, u32[]{:S(2)}) collective-permute-start(bf16[2048,256]{1,0:T(8,128)(2,1)S(1)} %pad_maximum_fusion.refs_0_), channel_id=1, source_target_pairs={{0,1},{1,0},{2,3},{3,2},{4,5},{5,4},{6,7},{7,6},{8,9},{9,8},{10,11... | collective-permute-start | bytes 3145736 | tf_op jit(solution)/shard_map/ppermute | solution.py:30
  58.7 1.9 %collective-permute-start.7 = (bf16[2048,256]{1,0:T(8,128)(2,1)S(1)}, bf16[2048,256]{1,0:T(8,128)(2,1)}, u32[]{:S(2)}, u32[]{:S(2)}) collective-permute-start(bf16[2048,256]{1,0:T(8,128)(2,1)S(1)} %collective-permute-done.6.refs_2_), channel_id=1, source_target_pairs={{0,1},{1,0},{2,3},{3,2},{4,5},{5,4},{6,7},{7,6},{8,9},{9,8},{10,11... | collective-permute-start | bytes 3145736 | tf_op jit(solution)/shard_map/ppermute | solution.py:30
  60.6 2.4 %collective-permute-start.8 = (bf16[128,2048]{1,0:T(8,128)(2,1)}, bf16[128,2048]{1,0:T(8,128)(2,1)}, u32[]{:S(2)}, u32[]{:S(2)}) collective-permute-start(bf16[128,2048]{1,0:T(8,128)(2,1)} %bitcast.121), channel_id=1, source_target_pairs={{0,1},{1,0},{2,3},{3,2},{4,5},{5,4},{6,7},{7,6},{8,9},{9,8},{10,11... | collective-permute-start | bytes 1572872 | tf_op jit(solution)/shard_map/ppermute | solution.py:30
  63.1 4.8 %collective-permute-done.9.refs_6_ = bf16[128,2048]{1,0:T(8,128)(2,1)} collective-permute-done((bf16[128,2048]{1,0:T(8,128)(2,1)}, bf16[128,2048]{1,0:T(8,128)(2,1)}, u32[]{:S(2)}, u32[]{:S(2)}) %collective-permute-start.9) | collective-permute-done | bytes 524320 | tf_op jit(solution)/shard_map/ppermute | solution.py:30
  67.9 3.4 %collective-permute-start.10 = (bf16[128,2048]{1,0:T(8,128)(2,1)}, bf16[128,2048]{1,0:T(8,128)(2,1)}, u32[]{:S(2)}, u32[]{:S(2)}) collective-permute-start(bf16[128,2048]{1,0:T(8,128)(2,1)} %collective-permute-done.9.refs_6_), channel_id=1, source_target_pairs={{0,1},{1,0},{2,3},{3,2},{4,5},{5,4},{6,7},{7,6},{8,9},{9,8},{10,11... | collective-permute-start | bytes 1572872 | tf_op jit(solution)/shard_map/ppermute | solution.py:30
  71.3 0.6 reduce_sum.61
  71.9 1.3 fusion.55
  73.2 1.2 multiply_bitcast_fusion
  74.3 4.8 %all-to-all-done.1 = bf16[32,8,2048]{2,1,0:T(8,128)(2,1)S(1)} async-done(((bf16[32,8,2048]{2,1,0:T(8,128)(2,1)}), bf16[32,8,2048]{2,1,0:T(8,128)(2,1)S(1)}, u32[]{:S(2)}, u32[]{:S(2)}) %all-to-all-start.1) | async-done | bytes 1048608 | tf_op jit(solution)/shard_map/all_to_all | solution.py:34
  79.2 1.0 copy-done.2
  80.2 6.3 %expert.1 = bf16[256,2048]{1,0:T(8,128)(2,1)} custom-call(bf16[256,2048]{1,0:T(8,128)(2,1)} %bitcast.116, bf16[2048,256]{1,0:T(8,128)(2,1)} %copy-done.1, bf16[2048,256]{1,0:T(8,128)(2,1)} %collective-permute-done.5.refs_1_, bf16[2048,256]{1,0:T(8,128)(2,1)} %copy-done.4, bf16[2048,256]{1,0:T(8,128)(2,1)} %collective-permute-done.7.refs_3_, ...), custom_call_target="tpu_custom_call" | custom-call | tf_op jit(solution)/shard_map/expert/pallas_call | solution.py:194
  86.5 6.3 %all-to-all-start.2 = ((bf16[32,8,2048]{2,1,0:T(8,128)(2,1)}), bf16[32,8,2048]{2,1,0:T(8,128)(2,1)S(1)}, u32[]{:S(2)}, u32[]{:S(2)}) async-start(bf16[32,8,2048]{2,1,0:T(8,128)(2,1)} %bitcast.115), calls=%async_computation.2 | async-start | bytes 2097152 | tf_op jit(solution)/shard_map/all_to_all | solution.py:34
  92.9 0.4 fusion.20
  93.4 3.8 %collective-permute-start.1 = (bf16[2,2,2,8,2048]{4,3,0,1,2:T(8,128)(2,1)S(1)}, bf16[2,2,2,8,2048]{4,3,0,1,2:T(8,128)(2,1)S(1)}, u32[]{:S(2)}, u32[]{:S(2)}) collective-permute-start(bf16[2,2,2,8,2048]{4,3,0,1,2:T(8,128)(2,1)S(1)} %fusion.15), channel_id=1, source_target_pairs={{0,1},{1,0},{2,3},{3,2},{4,5},{5,4},{6,7},{7,6},{8,9},{9,8},{10,11... | collective-permute-start | bytes 786440 | tf_op jit(solution)/shard_map/ppermute | solution.py:30
  97.2 1.1 collective-permute-done.1
  98.4 3.0 %collective-permute-start.2 = (bf16[2,2,8,2048]{3,2,0,1:T(8,128)(2,1)S(1)}, bf16[2,2,8,2048]{3,2,0,1:T(8,128)(2,1)S(1)}, u32[]{:S(2)}, u32[]{:S(2)}) collective-permute-start(bf16[2,2,8,2048]{3,2,0,1:T(8,128)(2,1)S(1)} %fusion.16), channel_id=1, source_target_pairs={{0,2},{2,0},{1,3},{3,1},{4,6},{6,4},{5,7},{7,5},{8,10},{10,8},{9,1... | collective-permute-start | bytes 393224 | tf_op jit(solution)/shard_map/ppermute | solution.py:30
  101.4 3.6 %collective-permute-done.2 = bf16[2,2,8,2048]{3,2,0,1:T(8,128)(2,1)S(1)} collective-permute-done((bf16[2,2,8,2048]{3,2,0,1:T(8,128)(2,1)S(1)}, bf16[2,2,8,2048]{3,2,0,1:T(8,128)(2,1)S(1)}, u32[]{:S(2)}, u32[]{:S(2)}) %collective-permute-start.2) | collective-permute-done | bytes 131104 | tf_op jit(solution)/shard_map/ppermute | solution.py:30
  105.1 3.0 %collective-permute-start.3 = (bf16[2,8,2048]{2,1,0:T(8,128)(2,1)S(1)}, bf16[2,8,2048]{2,1,0:T(8,128)(2,1)S(1)}, u32[]{:S(2)}, u32[]{:S(2)}) collective-permute-start(bf16[2,8,2048]{2,1,0:T(8,128)(2,1)S(1)} %fusion.17), channel_id=1, source_target_pairs={{0,4},{4,0},{1,5},{5,1},{2,6},{6,2},{3,7},{7,3},{8,12},{12,8},{9,1... | collective-permute-start | bytes 196616 | tf_op jit(solution)/shard_map/ppermute | solution.py:30
  108.1 10.3 %all-to-all-done.2 = bf16[32,8,2048]{2,1,0:T(8,128)(2,1)S(1)} async-done(((bf16[32,8,2048]{2,1,0:T(8,128)(2,1)}), bf16[32,8,2048]{2,1,0:T(8,128)(2,1)S(1)}, u32[]{:S(2)}, u32[]{:S(2)}) %all-to-all-start.2) | async-done | bytes 1048608 | tf_op jit(solution)/shard_map/all_to_all | solution.py:34
  118.4 0.3 fusion.12
  118.7 0.5 copy-done.9
  119.2 1.1 fusion.1
  120.3 6.9 %all-to-all-start.3 = ((bf16[16,8,2048]{2,1,0:T(8,128)(2,1)}), bf16[16,8,2048]{2,1,0:T(8,128)(2,1)S(1)}, u32[]{:S(2)}, u32[]{:S(2)}) async-start(bf16[16,8,2048]{2,1,0:T(8,128)(2,1)} %fusion.1), calls=%async_computation.3 | async-start | bytes 1048576 | tf_op jit(solution)/shard_map/all_to_all | solution.py:34
  127.3 7.2 %collective-permute-start.4 = (bf16[8,2048]{1,0:T(8,128)(2,1)S(1)}, bf16[8,2048]{1,0:T(8,128)(2,1)S(1)}, u32[]{:S(2)}, u32[]{:S(2)}) collective-permute-start(bf16[8,2048]{1,0:T(8,128)(2,1)S(1)} %fusion.19), channel_id=1, source_target_pairs={{0,8},{8,0},{1,9},{9,1},{2,10},{10,2},{3,11},{11,3},{4,12},{12,4},... | collective-permute-start | bytes 98312 | tf_op jit(solution)/shard_map/ppermute | solution.py:30
  134.5 11.1 %collective-permute-done.4 = bf16[8,2048]{1,0:T(8,128)(2,1)S(1)} collective-permute-done((bf16[8,2048]{1,0:T(8,128)(2,1)S(1)}, bf16[8,2048]{1,0:T(8,128)(2,1)S(1)}, u32[]{:S(2)}, u32[]{:S(2)}) %collective-permute-start.4) | collective-permute-done | bytes 32800 | tf_op jit(solution)/shard_map/ppermute | solution.py:30
  145.6 17.4 %all_gather.6 = bf16[128,2048]{1,0:T(8,128)(2,1)S(1)} all-gather(bf16[8,2048]{1,0:T(8,128)(2,1)S(1)} %fusion.18), channel_id=1, replica_groups=mesh['ep'=32,'y2'=2,'y1'=2,'y0'=2,'c'=2] {'y2','y1','y0','c'}, dimensions={0}, use_global_device_ids=true | all-gather | bytes 557056 | tf_op jit(solution)/shard_map/all_gather | solution.py:38
  163.0 0.1 reduce_sum.62
  163.1 17.0 %all_gather.7 = bf16[128,2048]{1,0:T(8,128)(2,1)S(1)} all-gather(bf16[8,2048]{1,0:T(8,128)(2,1)S(1)} %reduce_sum.62), channel_id=1, replica_groups=mesh['ep'=32,'y2'=2,'y1'=2,'y0'=2,'c'=2] {'y2','y1','y0','c'}, dimensions={0}, use_global_device_ids=true | all-gather | bytes 557056 | tf_op jit(solution)/shard_map/all_gather | solution.py:38
  180.1 0.8 copy.33
  180.9 0.8 copy.34
  (50 shorter events, 0.3 us)
Async XLA Ops:
  0.6 92.2 %copy-start = (bf16[96,2048]{1,0:T(8,128)(2,1)S(1)}, bf16[96,2048]{1,0:T(8,128)(2,1)}, u32[]{:S(2)}) copy-start(bf16[96,2048]{1,0:T(8,128)(2,1)} %param.20) | copy-start | bytes 1179652
  0.6 2.7 %copy-start.3 = (bf16[128,2048]{1,0:T(8,128)(2,1)S(1)}, bf16[128,2048]{1,0:T(8,128)(2,1)}, u32[]{:S(2)}) copy-start(bf16[128,2048]{1,0:T(8,128)(2,1)} %param.14) | copy-start | bytes 1572868
  0.7 2.7 %copy-start.16 = (f32[2048]{0:T(1024)S(1)}, f32[2048]{0:T(1024)}, u32[]{:S(2)}) copy-start(f32[2048]{0:T(1024)} %param.15) | copy-start | bytes 24580
  0.7 2.7 %copy-start.14 = (bf16[2048,96]{0,1:T(8,128)(2,1)S(1)}, bf16[2048,96]{0,1:T(8,128)(2,1)}, u32[]{:S(2)}) copy-start(bf16[2048,96]{0,1:T(8,128)(2,1)} %param.16) | copy-start | bytes 1179652
  2.0 1.8 %copy-start.15 = (bf16[2048,96]{0,1:T(8,128)(2,1)S(1)}, bf16[2048,96]{0,1:T(8,128)(2,1)}, u32[]{:S(2)}) copy-start(bf16[2048,96]{0,1:T(8,128)(2,1)} %param.17) | copy-start | bytes 1179652
  3.8 4.5 %copy-start.5 = (bf16[1,2048,128]{2,1,0:T(8,128)(2,1)S(1)}, bf16[1,2048,128]{2,1,0:T(8,128)(2,1)}, u32[]{:S(2)}) copy-start(bf16[1,2048,128]{2,1,0:T(8,128)(2,1)} %param.26) | copy-start | bytes 1572868
  3.8 4.5 %copy-start.6 = (bf16[1,2048,128]{2,1,0:T(8,128)(2,1)S(1)}, bf16[1,2048,128]{2,1,0:T(8,128)(2,1)}, u32[]{:S(2)}) copy-start(bf16[1,2048,128]{2,1,0:T(8,128)(2,1)} %param.25) | copy-start | bytes 1572868
  4.3 7.4 %collective-permute-start = (bf16[30,96]{0,1:T(8,128)(2,1)S(1)}, bf16[30,96]{0,1:T(8,128)(2,1)S(1)}, u32[]{:S(2)}, u32[]{:S(2)}) collective-permute-start(bf16[30,96]{0,1:T(8,128)(2,1)S(1)} %slice.256), channel_id=1, source_target_pairs={{0,16},{16,32},{32,48},{48,64},{64,80},{80,96},{96,112},{112,128},... | collective-permute-start | bytes 17288 | tf_op jit(solution)/shard_map/ppermute | solution.py:26
  8.3 3.4 %copy-start.10 = (f32[31,96]{1,0:T(8,128)S(1)}, f32[31,96]{1,0:T(8,128)}, u32[]{:S(2)}) copy-start(f32[31,96]{1,0:T(8,128)} %param.18) | copy-start | bytes 35716
  8.4 47.4 %copy-start.1 = (bf16[2048,256]{1,0:T(8,128)(2,1)}, bf16[2048,256]{1,0:T(8,128)(2,1)S(1)}, u32[]{:S(2)}) copy-start(bf16[2048,256]{1,0:T(8,128)(2,1)S(1)} %pad_maximum_fusion.refs_0_) | copy-start | bytes 3145732
  8.4 50.3 %collective-permute-start.6 = (bf16[2048,256]{1,0:T(8,128)(2,1)S(1)}, bf16[2048,256]{1,0:T(8,128)(2,1)S(1)}, u32[]{:S(2)}, u32[]{:S(2)}) collective-permute-start(bf16[2048,256]{1,0:T(8,128)(2,1)S(1)} %pad_maximum_fusion.refs_0_), channel_id=1, source_target_pairs={{0,2},{2,0},{1,3},{3,1},{4,6},{6,4},{5,7},{7,5},{8,10},{10,8},{9,1... | collective-permute-start | bytes 3145736 | tf_op jit(solution)/shard_map/ppermute | solution.py:30
  13.8 26.4 %all-to-all-start = ((f32[16,2,128]{2,1,0:T(2,128)}), f32[16,2,128]{2,1,0:T(2,128)S(1)}, u32[]{:S(2)}, u32[]{:S(2)}) async-start(f32[16,2,128]{2,1,0:T(2,128)} %broadcast_in_dim.2), calls=%async_computation | async-start | bytes 32768 | tf_op jit(solution)/shard_map/all_to_all | solution.py:34
  40.2 38.9 %all-to-all-start.1 = ((bf16[32,8,2048]{2,1,0:T(8,128)(2,1)}), bf16[32,8,2048]{2,1,0:T(8,128)(2,1)S(1)}, u32[]{:S(2)}, u32[]{:S(2)}) async-start(bf16[32,8,2048]{2,1,0:T(8,128)(2,1)} %bitcast.119), calls=%async_computation.1 | async-start | bytes 2097152 | tf_op jit(solution)/shard_map/all_to_all | solution.py:34
  52.8 15.0 %collective-permute-start.9 = (bf16[128,2048]{1,0:T(8,128)(2,1)}, bf16[128,2048]{1,0:T(8,128)(2,1)}, u32[]{:S(2)}, u32[]{:S(2)}) collective-permute-start(bf16[128,2048]{1,0:T(8,128)(2,1)} %bitcast.120), channel_id=1, source_target_pairs={{0,2},{2,0},{1,3},{3,1},{4,6},{6,4},{5,7},{7,5},{8,10},{10,8},{9,1... | collective-permute-start | bytes 1572872 | tf_op jit(solution)/shard_map/ppermute | solution.py:30
  55.8 18.5 %collective-permute-start.5 = (bf16[2048,256]{1,0:T(8,128)(2,1)S(1)}, bf16[2048,256]{1,0:T(8,128)(2,1)}, u32[]{:S(2)}, u32[]{:S(2)}) collective-permute-start(bf16[2048,256]{1,0:T(8,128)(2,1)S(1)} %pad_maximum_fusion.refs_0_), channel_id=1, source_target_pairs={{0,1},{1,0},{2,3},{3,2},{4,5},{5,4},{6,7},{7,6},{8,9},{9,8},{10,11... | collective-permute-start | bytes 3145736 | tf_op jit(solution)/shard_map/ppermute | solution.py:30
  58.7 20.5 %copy-start.4 = (bf16[2048,256]{1,0:T(8,128)(2,1)}, bf16[2048,256]{1,0:T(8,128)(2,1)S(1)}, u32[]{:S(2)}) copy-start(bf16[2048,256]{1,0:T(8,128)(2,1)S(1)} %collective-permute-done.6.refs_2_) | copy-start | bytes 3145732
  58.7 20.5 %collective-permute-start.7 = (bf16[2048,256]{1,0:T(8,128)(2,1)S(1)}, bf16[2048,256]{1,0:T(8,128)(2,1)}, u32[]{:S(2)}, u32[]{:S(2)}) collective-permute-start(bf16[2048,256]{1,0:T(8,128)(2,1)S(1)} %collective-permute-done.6.refs_2_), channel_id=1, source_target_pairs={{0,1},{1,0},{2,3},{3,2},{4,5},{5,4},{6,7},{7,6},{8,9},{9,8},{10,11... | collective-permute-start | bytes 3145736 | tf_op jit(solution)/shard_map/ppermute | solution.py:30
  60.6 13.7 %collective-permute-start.8 = (bf16[128,2048]{1,0:T(8,128)(2,1)}, bf16[128,2048]{1,0:T(8,128)(2,1)}, u32[]{:S(2)}, u32[]{:S(2)}) collective-permute-start(bf16[128,2048]{1,0:T(8,128)(2,1)} %bitcast.121), channel_id=1, source_target_pairs={{0,1},{1,0},{2,3},{3,2},{4,5},{5,4},{6,7},{7,6},{8,9},{9,8},{10,11... | collective-permute-start | bytes 1572872 | tf_op jit(solution)/shard_map/ppermute | solution.py:30
  67.9 6.5 %collective-permute-start.10 = (bf16[128,2048]{1,0:T(8,128)(2,1)}, bf16[128,2048]{1,0:T(8,128)(2,1)}, u32[]{:S(2)}, u32[]{:S(2)}) collective-permute-start(bf16[128,2048]{1,0:T(8,128)(2,1)} %collective-permute-done.9.refs_6_), channel_id=1, source_target_pairs={{0,1},{1,0},{2,3},{3,2},{4,5},{5,4},{6,7},{7,6},{8,9},{9,8},{10,11... | collective-permute-start | bytes 1572872 | tf_op jit(solution)/shard_map/ppermute | solution.py:30
  79.2 1.0 copy-start.2
  86.5 6.4 %copy-start.7 = (f32[128,96]{0,1:T(8,128)S(1)}, f32[128,96]{0,1:T(8,128)}, u32[]{:S(2)}) copy-start(f32[128,96]{0,1:T(8,128)} %get-tuple-element.10) | copy-start | bytes 147460
  86.5 6.4 %copy-start.11 = (f32[96]{0:T(128)S(1)}, f32[96]{0:T(128)}, u32[]{:S(2)}) copy-start(f32[96]{0:T(128)} %param.19) | copy-start | bytes 1156
  86.5 6.4 %copy-start.12 = (f32[128]{0:T(128)S(1)}, f32[128]{0:T(128)}, u32[]{:S(2)}) copy-start(f32[128]{0:T(128)} %fusion.55) | copy-start | bytes 1540
  86.5 6.4 %copy-start.13 = (f32[128]{0:T(128)S(1)}, f32[128]{0:T(128)}, u32[]{:S(2)}) copy-start(f32[128]{0:T(128)} %multiply_bitcast_fusion) | copy-start | bytes 1540
  86.5 31.8 %all-to-all-start.2 = ((bf16[32,8,2048]{2,1,0:T(8,128)(2,1)}), bf16[32,8,2048]{2,1,0:T(8,128)(2,1)S(1)}, u32[]{:S(2)}, u32[]{:S(2)}) async-start(bf16[32,8,2048]{2,1,0:T(8,128)(2,1)} %bitcast.115), calls=%async_computation.2 | async-start | bytes 2097152 | tf_op jit(solution)/shard_map/all_to_all | solution.py:34
  93.4 5.0 %collective-permute-start.1 = (bf16[2,2,2,8,2048]{4,3,0,1,2:T(8,128)(2,1)S(1)}, bf16[2,2,2,8,2048]{4,3,0,1,2:T(8,128)(2,1)S(1)}, u32[]{:S(2)}, u32[]{:S(2)}) collective-permute-start(bf16[2,2,2,8,2048]{4,3,0,1,2:T(8,128)(2,1)S(1)} %fusion.15), channel_id=1, source_target_pairs={{0,1},{1,0},{2,3},{3,2},{4,5},{5,4},{6,7},{7,6},{8,9},{9,8},{10,11... | collective-permute-start | bytes 786440 | tf_op jit(solution)/shard_map/ppermute | solution.py:30
  98.4 20.0 %copy-start.8 = (bf16[256,128]{1,0:T(8,128)(2,1)S(1)}, bf16[256,128]{1,0:T(8,128)(2,1)}, u32[]{:S(2)}) copy-start(bf16[256,128]{1,0:T(8,128)(2,1)} %get-tuple-element.7) | copy-start | bytes 196612
  98.4 6.6 %collective-permute-start.2 = (bf16[2,2,8,2048]{3,2,0,1:T(8,128)(2,1)S(1)}, bf16[2,2,8,2048]{3,2,0,1:T(8,128)(2,1)S(1)}, u32[]{:S(2)}, u32[]{:S(2)}) collective-permute-start(bf16[2,2,8,2048]{3,2,0,1:T(8,128)(2,1)S(1)} %fusion.16), channel_id=1, source_target_pairs={{0,2},{2,0},{1,3},{3,1},{4,6},{6,4},{5,7},{7,5},{8,10},{10,8},{9,1... | collective-permute-start | bytes 393224 | tf_op jit(solution)/shard_map/ppermute | solution.py:30
  105.1 22.1 %collective-permute-start.3 = (bf16[2,8,2048]{2,1,0:T(8,128)(2,1)S(1)}, bf16[2,8,2048]{2,1,0:T(8,128)(2,1)S(1)}, u32[]{:S(2)}, u32[]{:S(2)}) collective-permute-start(bf16[2,8,2048]{2,1,0:T(8,128)(2,1)S(1)} %fusion.17), channel_id=1, source_target_pairs={{0,4},{4,0},{1,5},{5,1},{2,6},{6,2},{3,7},{7,3},{8,12},{12,8},{9,1... | collective-permute-start | bytes 196616 | tf_op jit(solution)/shard_map/ppermute | solution.py:30
  118.4 0.8 copy-start.9
  120.3 42.6 %all-to-all-start.3 = ((bf16[16,8,2048]{2,1,0:T(8,128)(2,1)}), bf16[16,8,2048]{2,1,0:T(8,128)(2,1)S(1)}, u32[]{:S(2)}, u32[]{:S(2)}) async-start(bf16[16,8,2048]{2,1,0:T(8,128)(2,1)} %fusion.1), calls=%async_computation.3 | async-start | bytes 1048576 | tf_op jit(solution)/shard_map/all_to_all | solution.py:34
  127.3 18.4 %collective-permute-start.4 = (bf16[8,2048]{1,0:T(8,128)(2,1)S(1)}, bf16[8,2048]{1,0:T(8,128)(2,1)S(1)}, u32[]{:S(2)}, u32[]{:S(2)}) collective-permute-start(bf16[8,2048]{1,0:T(8,128)(2,1)S(1)} %fusion.19), channel_id=1, source_target_pairs={{0,8},{8,0},{1,9},{9,1},{2,10},{10,2},{3,11},{11,3},{4,12},{12,4},... | collective-permute-start | bytes 98312 | tf_op jit(solution)/shard_map/ppermute | solution.py:30

commit v2 on v1

v2 whole, which is shorter than its diff:
```python
import jax
import jax.numpy as jnp
from jax import lax
from jax.experimental import pallas as pl
from jax.experimental.pallas import tpu as pltpu
from jax.sharding import Mesh
from jax.sharding import PartitionSpec as P

CONV_CH = 1536
CONV_W = 31
TOP_K = 4
BITS = ("y2", "y1", "y0", "c")
TP = BITS
GROUP = 4
EXPERTS = 32


epsilon = 1e-05
clamp_limit = 7.0
swish_slope = 1.702


def shifted(block, axis, distance):
    devices = range(lax.axis_size(axis))
    route = [(i - distance, i) for i in devices if i - distance in devices]
    return lax.ppermute(block, axis, route)


def swapped(x, axis):
    return lax.ppermute(x, axis, [(0, 1), (1, 0)])


def exchanged(x, axis):
    return lax.all_to_all(x, axis, split_axis=0, concat_axis=0, tiled=True)


def halved(x, axes):
    rows, width = x.shape
    sizes = [2] * len(axes)
    share = rows >> len(axes)
    for at in reversed(range(len(axes))):
        x = x.reshape(*sizes[: at + 1], share, width)
        own = lax.axis_index(axes[at])
        kept = lax.dynamic_index_in_dim(x, own, at, keepdims=False)
        given = lax.dynamic_index_in_dim(x, 1 - own, at, keepdims=False)
        x = kept + swapped(given.astype(jnp.bfloat16), axes[at]).astype(jnp.float32)
    return x.reshape(share, width)


def three_terms(x):
    terms = []
    for _ in range(3):
        term = x.astype(jnp.bfloat16)
        x = x - term.astype(jnp.float32)
        terms.append(term)
    return terms


def row_norm(inputs, gains):
    widened = inputs.astype(jnp.float32)
    row_mean = jnp.mean(widened, axis=-1, keepdims=True)
    row_var = jnp.mean(jnp.square(widened - row_mean), axis=-1, keepdims=True)
    return (widened - row_mean) * lax.rsqrt(row_var + epsilon) * gains


def packing_kernel(w_ref, gain_ref, out_ref):
    size, padded, step = out_ref.shape
    own = w_ref.shape[0]
    terms = three_terms(gain_ref[...])
    for block in range(size):
        out_ref[block, :own, :] = w_ref[:, block * step : (block + 1) * step]
        out_ref[block, own:, :] = jnp.zeros((padded - own, step), jnp.bfloat16)
        for at, term in enumerate(terms):
            out_ref[block, own + at : own + at + 1, :own] = term


def resharded(w_output, channel_gain):
    size = lax.axis_size(TP)
    own, width = w_output.shape
    step = width // size
    whole = pl.BlockSpec(memory_space=pltpu.VMEM)
    payload = pl.pallas_call(
        packing_kernel,
        in_specs=[whole] * 2,
        out_specs=whole,
        out_shape=jax.ShapeDtypeStruct((size, own + 8, step), jnp.bfloat16),
        name="packing",
    )(w_output, channel_gain.reshape(1, own))
    arrived = exchanged(payload, TP)
    columns = arrived[:, :own].reshape(size * own, step)
    terms = arrived[:, own : own + 3, :own].astype(jnp.float32)
    return columns, (terms[:, 0] + terms[:, 1] + terms[:, 2]).reshape(size * own, 1)


def convolved(mixer_in, mixer_gain, w_value, w_gate, w_taps):
    normed = row_norm(mixer_in, mixer_gain).astype(jnp.bfloat16)
    values = jnp.dot(normed, w_value, preferred_element_type=jnp.float32)
    gate_pre = jnp.dot(normed, w_gate, preferred_element_type=jnp.float32)
    gated_values = (values * jax.nn.sigmoid(gate_pre)).astype(jnp.bfloat16)
    mixer_rows = gated_values.shape[0]
    reach_rows = CONV_W - 1
    earlier = shifted(gated_values[mixer_rows - reach_rows :], "ep", 1)
    extended = jnp.concatenate([earlier, gated_values], axis=0)
    conv_out = jnp.zeros(gated_values.shape, jnp.float32)
    for offset in range(CONV_W):
        conv_out = (
            conv_out + extended[offset : offset + mixer_rows].astype(jnp.float32) * w_taps[offset]
        )
    return conv_out


def mixed_channels(conv_out, gains, columns):
    wide = conv_out.astype(jnp.float32)
    row_mean = jnp.sum(wide, axis=0, keepdims=True) / CONV_CH
    row_var = jnp.sum(wide * wide, axis=0, keepdims=True) / CONV_CH - row_mean * row_mean
    activated = jax.nn.silu((wide - row_mean) * lax.rsqrt(row_var + epsilon) * gains)
    return lax.dot_general(
        activated.astype(jnp.bfloat16),
        columns,
        (((0,), (0,)), ((), ())),
        preferred_element_type=jnp.float32,
    ).astype(jnp.bfloat16)


def places(ids_ref, rows):
    names = lax.broadcasted_iota(jnp.int32, (EXPERTS, rows), 0)
    named = [ids_ref[pl.ds(k, 1), :] == names for k in range(TOP_K)]
    chosen = jnp.zeros((EXPERTS, rows), jnp.float32)
    for k in range(TOP_K):
        chosen = jnp.where(named[k], 1.0, chosen)
    earlier = lax.broadcasted_iota(jnp.int32, (rows, rows), 0)
    later = lax.broadcasted_iota(jnp.int32, (rows, rows), 1)
    before = jnp.where(earlier < later, 1.0, 0.0).astype(jnp.bfloat16)
    rank = jnp.dot(chosen.astype(jnp.bfloat16), before, preferred_element_type=jnp.float32)
    return named, jnp.where(chosen > 0.0, rank, -1.0).astype(jnp.bfloat16)


def spread_over(sent, per_expert):
    of_row = lax.broadcasted_iota(jnp.int32, (sent, EXPERTS), 0) // per_expert
    of_col = lax.broadcasted_iota(jnp.int32, (sent, EXPERTS), 1)
    return jnp.where(of_row == of_col, 1.0, 0.0).astype(jnp.bfloat16)


def taken_by(place, spread, slots, member):
    sent, rows = spread.shape[0], place.shape[1]
    slot = lax.broadcasted_iota(jnp.int32, (sent, rows), 0) % slots * GROUP + member
    return jnp.dot(spread, place, preferred_element_type=jnp.float32) == slot.astype(jnp.float32)


def front_kernel(member, x_ref, gain_ref, ids_ref, rows_ref):
    rows = x_ref.shape[0]
    sent = rows_ref.shape[0]
    slots = sent // EXPERTS
    normed = row_norm(x_ref[...], gain_ref[...]).astype(jnp.bfloat16)
    _, place = places(ids_ref, rows)
    taken = taken_by(place, spread_over(sent, slots), slots, member[0])
    select = jnp.where(taken, 1.0, 0.0).astype(jnp.bfloat16)
    rows_ref[...] = jnp.dot(select, normed, preferred_element_type=jnp.float32).astype(jnp.bfloat16)


def front(member, x, gain, ids, sent):
    _, width = x.shape
    whole = pl.BlockSpec(memory_space=pltpu.VMEM)
    return pl.pallas_call(
        front_kernel,
        in_specs=[pl.BlockSpec(memory_space=pltpu.SMEM)] + [whole] * 3,
        out_specs=whole,
        out_shape=jax.ShapeDtypeStruct((sent, width), jnp.bfloat16),
        name="front",
    )(member.reshape(1), x, gain.reshape(1, width), ids)


def mixing_kernel(member, ids_ref, scores_ref, hi_ref, lo_ref):
    sent, rows = hi_ref.shape
    per_expert = sent // EXPERTS
    raised = [jnp.exp(scores_ref[pl.ds(k, 1), :]) for k in range(TOP_K)]
    total = raised[0] + raised[1] + raised[2] + raised[3]
    named, place = places(ids_ref, rows)
    weights = jnp.zeros((EXPERTS, rows), jnp.float32)
    for k in range(TOP_K):
        weights = jnp.where(named[k], raised[k] / total, weights)
    weights_hi = weights.astype(jnp.bfloat16)
    weights_lo = (weights - weights_hi.astype(jnp.float32)).astype(jnp.bfloat16)
    spread = spread_over(sent, per_expert)
    taken = taken_by(place, spread, per_expert // GROUP, member[0])
    wide_hi = jnp.dot(spread, weights_hi, preferred_element_type=jnp.float32)
    wide_lo = jnp.dot(spread, weights_lo, preferred_element_type=jnp.float32)
    hi_ref[...] = jnp.where(taken, wide_hi, 0.0).astype(jnp.bfloat16)
    lo_ref[...] = jnp.where(taken, wide_lo, 0.0).astype(jnp.bfloat16)


def mixing(member, ids, scores, sent):
    rows = ids.shape[1]
    whole = pl.BlockSpec(memory_space=pltpu.VMEM)
    return pl.pallas_call(
        mixing_kernel,
        in_specs=[pl.BlockSpec(memory_space=pltpu.SMEM)] + [whole] * 2,
        out_specs=[whole] * 2,
        out_shape=[jax.ShapeDtypeStruct((sent, rows), jnp.bfloat16)] * 2,
        name="mixing",
    )(member.reshape(1), ids, scores)


def expert_kernel(x_hbm, *refs):
    gus, downs, out_hbm = refs[:GROUP], refs[GROUP : 2 * GROUP], refs[2 * GROUP]
    x_buf, gu_buf, down_buf, out_buf, x_sem, gu_sem, down_sem, out_sem = refs[2 * GROUP + 1 :]
    inner = downs[0].shape[0]
    experts, parts, slots, step = out_hbm.shape
    x_copy = pltpu.make_async_copy(x_hbm, x_buf, x_sem)
    gu_copies = [pltpu.make_async_copy(gus[s], gu_buf.at[s], gu_sem.at[s]) for s in range(GROUP)]
    down_copies = [
        pltpu.make_async_copy(downs[s], down_buf.at[pl.ds(s * inner, inner)], down_sem.at[s])
        for s in range(GROUP)
    ]
    x_copy.start()
    gu_copies[0].start()
    gu_copies[1].start()
    x_copy.wait()
    hidden = []
    for s in range(GROUP):
        gu_copies[s].wait()
        if s + 2 < GROUP:
            gu_copies[s + 2].start()
        down_copies[s].start()
        both = jnp.dot(x_buf[...], gu_buf[s], preferred_element_type=jnp.float32)
        g = jnp.minimum(both[:, :inner], clamp_limit)
        u = jnp.clip(both[:, inner:], -clamp_limit, clamp_limit)
        hidden.append(((u + 1.0) * g * jax.nn.sigmoid(swish_slope * g)).astype(jnp.bfloat16))
    hidden = jnp.concatenate(hidden, axis=1)
    for copy in down_copies:
        copy.wait()
    out_copies = []
    for n in range(parts):
        product = jnp.dot(
            hidden, down_buf[:, n * step : (n + 1) * step], preferred_element_type=jnp.float32
        )
        out_buf[n] = product.reshape(experts, slots, step).astype(jnp.bfloat16)
        copy = pltpu.make_async_copy(out_buf.at[n], out_hbm.at[:, n], out_sem.at[n])
        copy.start()
        out_copies.append(copy)
    for copy in out_copies:
        copy.wait()


def expert(x, gus, downs):
    rows, width = x.shape
    inner = downs[0].shape[0]
    parts = GROUP
    step = width // parts
    slots = rows // EXPERTS
    outside = pl.BlockSpec(memory_space=pl.ANY)
    return pl.pallas_call(
        expert_kernel,
        in_specs=[outside] * (1 + 2 * GROUP),
        out_specs=outside,
        out_shape=jax.ShapeDtypeStruct((EXPERTS, parts, slots, step), jnp.bfloat16),
        scratch_shapes=[
            pltpu.VMEM((rows, width), jnp.bfloat16),
            pltpu.VMEM((GROUP, width, 2 * inner), jnp.bfloat16),
            pltpu.VMEM((GROUP * inner, width), jnp.bfloat16),
            pltpu.VMEM((parts, EXPERTS, slots, step), jnp.bfloat16),
            pltpu.SemaphoreType.DMA,
            pltpu.SemaphoreType.DMA((GROUP,)),
            pltpu.SemaphoreType.DMA((GROUP,)),
            pltpu.SemaphoreType.DMA((parts,)),
        ],
        name="expert",
    )(x, *gus, *downs)


def program(
    mixer_in,
    mixer_gain,
    w_value,
    w_gate,
    w_taps,
    channel_gain,
    w_output,
    expert_in,
    expert_gain,
    route_experts,
    route_scores,
    expert_gate,
    expert_up,
    expert_down,
):
    rows_b, width = expert_in.shape
    experts = lax.axis_size("ep")
    capacity = 2 * rows_b * TOP_K // experts
    slots = capacity // GROUP
    member = lax.axis_index(("y0", "c")).astype(jnp.int32)

    gate_up = jnp.concatenate([expert_gate[0], expert_up[0]], axis=1)
    down = expert_down[0]
    gu_y = swapped(gate_up, "y0")
    down_y = swapped(down, "y0")
    gu_c = swapped(gate_up, "c")
    down_c = swapped(down, "c")
    gu_d = swapped(gu_y, "c")
    down_d = swapped(down_y, "c")

    columns, gains = resharded(w_output, channel_gain)
    ids = route_experts.T
    sending = front(member, expert_in, expert_gain, ids, experts * slots)
    arrived = exchanged(sending.reshape(experts, slots, width), "ep").reshape(-1, width)

    mixing_hi, mixing_lo = mixing(member, ids, route_scores.T, experts * capacity)
    conv_out = convolved(mixer_in, mixer_gain, w_value, w_gate, w_taps)
    conv_all = lax.all_gather(conv_out.T.astype(jnp.bfloat16), TP, axis=0, tiled=True)
    mixer_share = mixed_channels(conv_all, gains, columns)
    mixer_out = lax.all_gather(mixer_share, TP)
    mixer_out = mixer_out.transpose(1, 0, 2).reshape(rows_b, width)

    partial = expert(arrived, (gate_up, gu_c, gu_y, gu_d), (down, down_c, down_y, down_d))
    wide = GROUP * experts
    returned = exchanged(partial.reshape(wide, slots, width // GROUP), ("ep", "y2", "y1"))
    returned = returned.reshape(wide * slots, width // GROUP)

    def mixed(m):
        return lax.dot_general(
            m, returned, (((0,), (0,)), ((), ())), preferred_element_type=jnp.float32
        )

    combined = mixed(mixing_hi) + mixed(mixing_lo)
    share = halved(combined, ("y0", "c")).astype(jnp.bfloat16)
    expert_out = lax.all_gather(share, TP)
    expert_out = expert_out.reshape(GROUP, rows_b, width // GROUP)
    expert_out = jnp.concatenate(list(expert_out), axis=1)
    return (mixer_out, expert_out)


def solution(mesh):
    split = Mesh(mesh.devices.reshape(mesh.shape["ep"], 2, 2, 2, 2), ("ep", *TP))
    in_specs = (
        P("ep", None),
        P(),
        P(None, TP),
        P(None, TP),
        P(None, TP),
        P(TP),
        P(TP, None),
        P("ep", None),
        P(),
        P("ep", None),
        P("ep", None),
        P("ep", None, TP),
        P("ep", None, TP),
        P("ep", TP, None),
    )
    out_specs = (P("ep", None), P("ep", None))
    return jax.shard_map(program, mesh=split, in_specs=in_specs, out_specs=out_specs, check_vma=False)
```

time: 183 us -> 173 us (0.945)
  the two profiles are of different devices: /device:TPU:1 before, /device:TPU:73 now
where the time goes in v2:
time: 173 us; the launch traced here: 172 us
  starting transfers between devices  63 us (36%)
  blocking collectives  51.8 us (30%)
  waiting for transfers between devices  35.4 us (20%)
  Pallas kernels  13.1 us (8%)
  local copies, waits for them, and re-layouts  3.15 us (2%)
  other arithmetic  2.55 us (1%)
  matrix products  2.07 us (1%)
    all_to_all x3, starting transfers between devices, exchanged(): return lax.all_to_all(x, axis, split_axis=0, concat_axis=0, tiled=True)  33.9 us
    ppermute x8, starting transfers between devices, swapped(): return lax.ppermute(x, axis, [(0, 1), (1, 0)])  26 us
    ppermute x8, waiting for transfers between devices, swapped(): return lax.ppermute(x, axis, [(0, 1), (1, 0)])  18.4 us
    all_gather x1, blocking collectives, program(): lax.all_gather(conv_out.T.astype(jnp.bfloat16), TP, axis=0, tiled=True)  18.3 us
    all_gather x1, blocking collectives, program(): expert_out = lax.all_gather(share, TP)  17.6 us
    ppermute x1, waiting for transfers between devices, shifted(): return lax.ppermute(block, axis, route)  16.9 us
    all_gather x1, blocking collectives, program(): mixer_out = lax.all_gather(mixer_share, TP)  15.9 us
    pallas_call x1, Pallas kernels, expert(): pl.pallas_call(expert_kernel, in_specs=[outside] * (1 + 2 * GROUP), out_s...  6.3 us
  transfers between devices with their start and end apart: 12, of which 4 were waited for; matrix products, arithmetic and copies ran while one was open for 2% of the time, Pallas kernels for 6%

profile of v2, /device:TPU:73, one launch (start us, length us, event | category | flops | bytes accessed | tf_op | source)
XLA Modules:
  0.0 172.0 jit_solution(16192901692784950667)
XLA Ops:
  0.6 0.0 copy-start
  0.7 2.9 %front.1 = bf16[256,2048]{1,0:T(8,128)(2,1)} custom-call(s32[1]{0:T(128)} %bitcast.36.member, bf16[128,2048]{1,0:T(8,128)(2,1)} %x_ref.1, f32[1,2048]{1,0:T(1,128)} %bitcast.118, s32[4,128]{1,0:T(4,128)} %bitcast.119), custom_call_target="tpu_custom_call" | custom-call | tf_op jit(solution)/shard_map/front/pallas_call | solution.py:164
  3.6 12.2 %all-to-all-start.1 = ((bf16[32,8,2048]{2,1,0:T(8,128)(2,1)}), bf16[32,8,2048]{2,1,0:T(8,128)(2,1)S(1)}, u32[]{:S(2)}, u32[]{:S(2)}) async-start(bf16[32,8,2048]{2,1,0:T(8,128)(2,1)} %bitcast.108), calls=%async_computation.1 | async-start | bytes 2097152 | tf_op jit(solution)/shard_map/all_to_all | solution.py:34
  15.8 0.1 pad_maximum_fusion.refs_0_
  15.9 0.0 copy-start.3
  15.9 2.2 %collective-permute-start.2 = (bf16[2048,256]{1,0:T(8,128)(2,1)S(1)}, bf16[2048,256]{1,0:T(8,128)(2,1)}, u32[]{:S(2)}, u32[]{:S(2)}) collective-permute-start(bf16[2048,256]{1,0:T(8,128)(2,1)S(1)} %pad_maximum_fusion.refs_0_), channel_id=1, source_target_pairs={{0,2},{2,0},{1,3},{3,1},{4,6},{6,4},{5,7},{7,5},{8,10},{10,8},{9,1... | collective-permute-start | bytes 3145736 | tf_op jit(solution)/shard_map/ppermute | solution.py:30
  18.1 3.2 %collective-permute-start.5 = (bf16[128,2048]{1,0:T(8,128)(2,1)}, bf16[128,2048]{1,0:T(8,128)(2,1)}, u32[]{:S(2)}, u32[]{:S(2)}) collective-permute-start(bf16[128,2048]{1,0:T(8,128)(2,1)} %bitcast.44.refs_4_), channel_id=1, source_target_pairs={{0,2},{2,0},{1,3},{3,1},{4,6},{6,4},{5,7},{7,5},{8,10},{10,8},{9,1... | collective-permute-start | bytes 1572872 | tf_op jit(solution)/shard_map/ppermute | solution.py:30
  21.3 3.7 %collective-permute-start.1 = (bf16[2048,256]{1,0:T(8,128)(2,1)S(1)}, bf16[2048,256]{1,0:T(8,128)(2,1)}, u32[]{:S(2)}, u32[]{:S(2)}) collective-permute-start(bf16[2048,256]{1,0:T(8,128)(2,1)S(1)} %pad_maximum_fusion.refs_0_), channel_id=1, source_target_pairs={{0,1},{1,0},{2,3},{3,2},{4,5},{5,4},{6,7},{7,6},{8,9},{9,8},{10,11... | collective-permute-start | bytes 3145736 | tf_op jit(solution)/shard_map/ppermute | solution.py:30
  25.0 16.5 %collective-permute-done.2.refs_2_ = bf16[2048,256]{1,0:T(8,128)(2,1)} collective-permute-done((bf16[2048,256]{1,0:T(8,128)(2,1)S(1)}, bf16[2048,256]{1,0:T(8,128)(2,1)}, u32[]{:S(2)}, u32[]{:S(2)}) %collective-permute-start.2) | collective-permute-done | bytes 1048608 | tf_op jit(solution)/shard_map/ppermute | solution.py:30
  41.5 5.7 %collective-permute-start.3 = (bf16[2048,256]{1,0:T(8,128)(2,1)}, bf16[2048,256]{1,0:T(8,128)(2,1)}, u32[]{:S(2)}, u32[]{:S(2)}) collective-permute-start(bf16[2048,256]{1,0:T(8,128)(2,1)} %collective-permute-done.2.refs_2_), channel_id=1, source_target_pairs={{0,1},{1,0},{2,3},{3,2},{4,5},{5,4},{6,7},{7,6},{8,9},{9,8},{10,11... | collective-permute-start | bytes 3145736 | tf_op jit(solution)/shard_map/ppermute | solution.py:30
  47.2 1.9 %packing.1 = bf16[16,104,128]{2,1,0:T(8,128)(2,1)} custom-call(bf16[96,2048]{1,0:T(8,128)(2,1)} %w_ref.1, f32[1,96]{1,0:T(1,128)} %bitcast.122), custom_call_target="tpu_custom_call" | custom-call | tf_op jit(solution)/shard_map/packing/pallas_call | solution.py:82
  49.1 0.0 all-to-all-done.1
  49.1 7.3 %all-to-all-start = ((bf16[16,104,128]{2,1,0:T(8,128)(2,1)}), bf16[16,104,128]{2,1,0:T(8,128)(2,1)S(1)}, u32[]{:S(2)}, u32[]{:S(2)}) async-start(bf16[16,104,128]{2,1,0:T(8,128)(2,1)} %packing.1), calls=%async_computation | async-start | bytes 851968 | tf_op jit(solution)/shard_map/all_to_all | solution.py:34
  56.4 2.3 %collective-permute-start.4 = (bf16[128,2048]{1,0:T(8,128)(2,1)}, bf16[128,2048]{1,0:T(8,128)(2,1)S(1)}, u32[]{:S(2)}, u32[]{:S(2)}) collective-permute-start(bf16[128,2048]{1,0:T(8,128)(2,1)} %bitcast.44.refs_4_), channel_id=1, source_target_pairs={{0,1},{1,0},{2,3},{3,2},{4,5},{5,4},{6,7},{7,6},{8,9},{9,8},{10,11... | collective-permute-start | bytes 1572872 | tf_op jit(solution)/shard_map/ppermute | solution.py:30
  58.7 2.0 %collective-permute-start.6 = (bf16[128,2048]{1,0:T(8,128)(2,1)}, bf16[128,2048]{1,0:T(8,128)(2,1)S(1)}, u32[]{:S(2)}, u32[]{:S(2)}) collective-permute-start(bf16[128,2048]{1,0:T(8,128)(2,1)} %collective-permute-done.5.refs_6_), channel_id=1, source_target_pairs={{0,1},{1,0},{2,3},{3,2},{4,5},{5,4},{6,7},{7,6},{8,9},{9,8},{10,11... | collective-permute-start | bytes 1572872 | tf_op jit(solution)/shard_map/ppermute | solution.py:30
  60.7 0.2 convert_reduce_fusion
  60.9 0.3 fusion.7
  61.2 0.0 copy-start.5
  61.2 1.5 collective-permute-done.6.refs_7_
  62.7 0.8 copy-done.6
  63.5 6.3 %expert.1 = bf16[32,4,8,512]{3,2,1,0:T(8,128)(2,1)} custom-call(bf16[256,2048]{1,0:T(8,128)(2,1)} %bitcast.110, bf16[2048,256]{1,0:T(8,128)(2,1)} %copy-done.2, bf16[2048,256]{1,0:T(8,128)(2,1)} %collective-permute-done.1.refs_1_, bf16[2048,256]{1,0:T(8,128)(2,1)} %collective-permute-done.2.refs_2_, bf16[2048,256]{1,0:T(8,128)(2,1)} %collective-permute-done.3.refs_3_, ...), custom_call_target="tpu_custom_call" | custom-call | tf_op jit(solution)/shard_map/expert/pallas_call | solution.py:252
  69.8 0.0 copy-start.4
  69.8 0.0 copy-start.13
  69.8 14.5 %all-to-all-start.2 = ((bf16[128,8,512]{2,1,0:T(8,128)(2,1)}), bf16[128,8,512]{2,1,0:T(8,128)(2,1)S(1)}, u32[]{:S(2)}, u32[]{:S(2)}) async-start(bf16[128,8,512]{2,1,0:T(8,128)(2,1)} %bitcast.109), calls=%async_computation.2 | async-start | bytes 2097152 | tf_op jit(solution)/shard_map/all_to_all | solution.py:34
  84.3 0.0 copy-start.12
  84.3 0.4 fusion.63
  84.7 0.6 copy-done.12
  85.3 0.4 fusion.6
  85.7 0.1 slice.276
  85.8 3.1 %collective-permute-start = (bf16[30,96]{0,1:T(8,128)(2,1)S(1)}, bf16[30,96]{0,1:T(8,128)(2,1)S(1)}, u32[]{:S(2)}, u32[]{:S(2)}) collective-permute-start(bf16[30,96]{0,1:T(8,128)(2,1)S(1)} %slice.276), channel_id=1, source_target_pairs={{0,16},{16,32},{32,48},{48,64},{64,80},{80,96},{96,112},{112,128},... | collective-permute-start | bytes 17288 | tf_op jit(solution)/shard_map/ppermute | solution.py:26
  88.9 2.0 %mixing.1 = (bf16[1024,128]{1,0:T(8,128)(2,1)}, bf16[1024,128]{1,0:T(8,128)(2,1)}) custom-call(s32[1]{0:T(128)} %bitcast.36.member, s32[4,128]{1,0:T(4,128)} %bitcast.120, f32[4,128]{1,0:T(4,128)} %bitcast.121), custom_call_target="tpu_custom_call" | custom-call | tf_op jit(solution)/shard_map/mixing/pallas_call | solution.py:195
  90.9 16.9 %collective-permute-done = bf16[30,96]{0,1:T(8,128)(2,1)S(1)} collective-permute-done((bf16[30,96]{0,1:T(8,128)(2,1)S(1)}, bf16[30,96]{0,1:T(8,128)(2,1)S(1)}, u32[]{:S(2)}, u32[]{:S(2)}) %collective-permute-start) | collective-permute-done | bytes 5792 | tf_op jit(solution)/shard_map/ppermute | solution.py:26
  107.9 0.8 fusion.59
  108.7 18.3 %all_gather.15 = bf16[1536,128]{1,0:T(8,128)(2,1)S(1)} all-gather(bf16[96,128]{1,0:T(8,128)(2,1)S(1)} %fusion.59), channel_id=1, replica_groups=mesh['ep'=32,'y2'=2,'y1'=2,'y0'=2,'c'=2] {'y2','y1','y0','c'}, dimensions={0}, use_global_device_ids=true | all-gather | bytes 417792 | tf_op jit(solution)/shard_map/all_gather | solution.py:309
  127.1 0.2 convert_reduce_fusion.1
  127.3 0.1 add.199
  127.4 0.3 fusion.10
  127.8 0.0 slice-start
  127.8 0.6 copy-done.9
  128.4 0.3 convolution_add_fusion
  128.7 2.1 %collective-permute-start.7 = (bf16[2,32,512]{2,1,0:T(8,128)(2,1)S(1)}, bf16[2,32,512]{2,1,0:T(8,128)(2,1)S(1)}, u32[]{:S(2)}, u32[]{:S(2)}) collective-permute-start(bf16[2,32,512]{2,1,0:T(8,128)(2,1)S(1)} %fusion.27), channel_id=1, source_target_pairs={{0,1},{1,0},{2,3},{3,2},{4,5},{5,4},{6,7},{7,6},{8,9},{9,8},{10,11... | collective-permute-start | bytes 196616 | tf_op jit(solution)/shard_map/ppermute | solution.py:30
  130.8 0.6 convolution_convert_fusion
  131.4 0.5 collective-permute-done.7
  131.9 4.8 %collective-permute-start.8 = (bf16[32,512]{1,0:T(8,128)(2,1)S(1)}, bf16[32,512]{1,0:T(8,128)(2,1)S(1)}, u32[]{:S(2)}, u32[]{:S(2)}) collective-permute-start(bf16[32,512]{1,0:T(8,128)(2,1)S(1)} %fusion.29), channel_id=1, source_target_pairs={{0,2},{2,0},{1,3},{3,1},{4,6},{6,4},{5,7},{7,5},{8,10},{10,8},{9,1... | collective-permute-start | bytes 98312 | tf_op jit(solution)/shard_map/ppermute | solution.py:30
  136.7 15.9 %all-gather = bf16[2048,128]{1,0:T(8,128)(2,1)S(1)} all-gather(bf16[128,128]{1,0:T(8,128)(2,1)S(1)} %convolution_convert_fusion), channel_id=2, replica_groups=mesh['ep'=32,'y2'=2,'y1'=2,'y0'=2,'c'=2] {'y2','y1','y0','c'}, dimensions={0}, use_global_device_ids=true | all-gather | bytes 557056 | tf_op jit(solution)/shard_map/all_gather | solution.py:311
  152.6 0.9 copy.21
  153.5 17.6 %all-gather.1 = bf16[512,512]{1,0:T(8,128)(2,1)S(1)} all-gather(bf16[32,512]{1,0:T(8,128)(2,1)S(1)} %fusion.28), channel_id=3, replica_groups=mesh['ep'=32,'y2'=2,'y1'=2,'y0'=2,'c'=2] {'y2','y1','y0','c'}, dimensions={0}, use_global_device_ids=true | all-gather | bytes 557056 | tf_op jit(solution)/shard_map/all_gather | solution.py:326
  171.1 0.8 pad_maximum_fusion.1
  (39 shorter events, 0.2 us)
Async XLA Ops:
  0.6 83.7 %copy-start = (bf16[2048,96]{0,1:T(8,128)(2,1)S(1)}, bf16[2048,96]{0,1:T(8,128)(2,1)}, u32[]{:S(2)}) copy-start(bf16[2048,96]{0,1:T(8,128)(2,1)} %param.16) | copy-start | bytes 1179652
  3.6 12.2 %copy-start.7 = (bf16[1,2048,128]{2,1,0:T(8,128)(2,1)S(1)}, bf16[1,2048,128]{2,1,0:T(8,128)(2,1)}, u32[]{:S(2)}) copy-start(bf16[1,2048,128]{2,1,0:T(8,128)(2,1)} %param.26) | copy-start | bytes 1572868
  3.6 12.2 %copy-start.8 = (bf16[1,2048,128]{2,1,0:T(8,128)(2,1)S(1)}, bf16[1,2048,128]{2,1,0:T(8,128)(2,1)}, u32[]{:S(2)}) copy-start(bf16[1,2048,128]{2,1,0:T(8,128)(2,1)} %param.25) | copy-start | bytes 1572868
  3.6 45.5 %all-to-all-start.1 = ((bf16[32,8,2048]{2,1,0:T(8,128)(2,1)}), bf16[32,8,2048]{2,1,0:T(8,128)(2,1)S(1)}, u32[]{:S(2)}, u32[]{:S(2)}) async-start(bf16[32,8,2048]{2,1,0:T(8,128)(2,1)} %bitcast.108), calls=%async_computation.1 | async-start | bytes 2097152 | tf_op jit(solution)/shard_map/all_to_all | solution.py:34
  15.9 45.0 %copy-start.2 = (bf16[2048,256]{1,0:T(8,128)(2,1)}, bf16[2048,256]{1,0:T(8,128)(2,1)S(1)}, u32[]{:S(2)}) copy-start(bf16[2048,256]{1,0:T(8,128)(2,1)S(1)} %pad_maximum_fusion.refs_0_) | copy-start | bytes 3145732
  15.9 44.8 %copy-start.3 = (bf16[128,2048]{1,0:T(8,128)(2,1)S(1)}, bf16[128,2048]{1,0:T(8,128)(2,1)}, u32[]{:S(2)}) copy-start(bf16[128,2048]{1,0:T(8,128)(2,1)} %param.14) | copy-start | bytes 1572868
  15.9 25.6 %collective-permute-start.2 = (bf16[2048,256]{1,0:T(8,128)(2,1)S(1)}, bf16[2048,256]{1,0:T(8,128)(2,1)}, u32[]{:S(2)}, u32[]{:S(2)}) collective-permute-start(bf16[2048,256]{1,0:T(8,128)(2,1)S(1)} %pad_maximum_fusion.refs_0_), channel_id=1, source_target_pairs={{0,2},{2,0},{1,3},{3,1},{4,6},{6,4},{5,7},{7,5},{8,10},{10,8},{9,1... | collective-permute-start | bytes 3145736 | tf_op jit(solution)/shard_map/ppermute | solution.py:30
  18.1 40.5 %collective-permute-start.5 = (bf16[128,2048]{1,0:T(8,128)(2,1)}, bf16[128,2048]{1,0:T(8,128)(2,1)}, u32[]{:S(2)}, u32[]{:S(2)}) collective-permute-start(bf16[128,2048]{1,0:T(8,128)(2,1)} %bitcast.44.refs_4_), channel_id=1, source_target_pairs={{0,2},{2,0},{1,3},{3,1},{4,6},{6,4},{5,7},{7,5},{8,10},{10,8},{9,1... | collective-permute-start | bytes 1572872 | tf_op jit(solution)/shard_map/ppermute | solution.py:30
  21.3 41.4 %collective-permute-start.1 = (bf16[2048,256]{1,0:T(8,128)(2,1)S(1)}, bf16[2048,256]{1,0:T(8,128)(2,1)}, u32[]{:S(2)}, u32[]{:S(2)}) collective-permute-start(bf16[2048,256]{1,0:T(8,128)(2,1)S(1)} %pad_maximum_fusion.refs_0_), channel_id=1, source_target_pairs={{0,1},{1,0},{2,3},{3,2},{4,5},{5,4},{6,7},{7,6},{8,9},{9,8},{10,11... | collective-permute-start | bytes 3145736 | tf_op jit(solution)/shard_map/ppermute | solution.py:30
  41.5 21.2 %collective-permute-start.3 = (bf16[2048,256]{1,0:T(8,128)(2,1)}, bf16[2048,256]{1,0:T(8,128)(2,1)}, u32[]{:S(2)}, u32[]{:S(2)}) collective-permute-start(bf16[2048,256]{1,0:T(8,128)(2,1)} %collective-permute-done.2.refs_2_), channel_id=1, source_target_pairs={{0,1},{1,0},{2,3},{3,2},{4,5},{5,4},{6,7},{7,6},{8,9},{9,8},{10,11... | collective-permute-start | bytes 3145736 | tf_op jit(solution)/shard_map/ppermute | solution.py:30
  49.1 14.4 %copy-start.1 = (bf16[32,8,2048]{2,1,0:T(8,128)(2,1)}, bf16[32,8,2048]{2,1,0:T(8,128)(2,1)S(1)}, u32[]{:S(2)}) copy-start(bf16[32,8,2048]{2,1,0:T(8,128)(2,1)S(1)} %all-to-all-done.1) | copy-start | bytes 3145732
  49.1 20.7 %all-to-all-start = ((bf16[16,104,128]{2,1,0:T(8,128)(2,1)}), bf16[16,104,128]{2,1,0:T(8,128)(2,1)S(1)}, u32[]{:S(2)}, u32[]{:S(2)}) async-start(bf16[16,104,128]{2,1,0:T(8,128)(2,1)} %packing.1), calls=%async_computation | async-start | bytes 851968 | tf_op jit(solution)/shard_map/all_to_all | solution.py:34
  56.4 4.8 %collective-permute-start.4 = (bf16[128,2048]{1,0:T(8,128)(2,1)}, bf16[128,2048]{1,0:T(8,128)(2,1)S(1)}, u32[]{:S(2)}, u32[]{:S(2)}) collective-permute-start(bf16[128,2048]{1,0:T(8,128)(2,1)} %bitcast.44.refs_4_), channel_id=1, source_target_pairs={{0,1},{1,0},{2,3},{3,2},{4,5},{5,4},{6,7},{7,6},{8,9},{9,8},{10,11... | collective-permute-start | bytes 1572872 | tf_op jit(solution)/shard_map/ppermute | solution.py:30
  58.7 4.0 %collective-permute-start.6 = (bf16[128,2048]{1,0:T(8,128)(2,1)}, bf16[128,2048]{1,0:T(8,128)(2,1)S(1)}, u32[]{:S(2)}, u32[]{:S(2)}) collective-permute-start(bf16[128,2048]{1,0:T(8,128)(2,1)} %collective-permute-done.5.refs_6_), channel_id=1, source_target_pairs={{0,1},{1,0},{2,3},{3,2},{4,5},{5,4},{6,7},{7,6},{8,9},{9,8},{10,11... | collective-permute-start | bytes 1572872 | tf_op jit(solution)/shard_map/ppermute | solution.py:30
  61.2 1.5 copy-start.5
  62.7 0.8 copy-start.6
  69.8 57.6 %copy-start.4 = (bf16[16,104,128]{2,1,0:T(8,128)(2,1)}, bf16[16,104,128]{2,1,0:T(8,128)(2,1)S(1)}, u32[]{:S(2)}) copy-start(bf16[16,104,128]{2,1,0:T(8,128)(2,1)S(1)} %all-to-all-done) | copy-start | bytes 1277956
  69.8 14.5 %copy-start.13 = (f32[2048]{0:T(1024)S(1)}, f32[2048]{0:T(1024)}, u32[]{:S(2)}) copy-start(f32[2048]{0:T(1024)} %param.15) | copy-start | bytes 24580
  69.8 57.6 %all-to-all-start.2 = ((bf16[128,8,512]{2,1,0:T(8,128)(2,1)}), bf16[128,8,512]{2,1,0:T(8,128)(2,1)S(1)}, u32[]{:S(2)}, u32[]{:S(2)}) async-start(bf16[128,8,512]{2,1,0:T(8,128)(2,1)} %bitcast.109), calls=%async_computation.2 | async-start | bytes 2097152 | tf_op jit(solution)/shard_map/all_to_all | solution.py:34
  84.3 1.0 copy-start.12
  85.3 3.6 %copy-start.11 = (f32[31,96]{1,0:T(8,128)S(1)}, f32[31,96]{1,0:T(8,128)}, u32[]{:S(2)}) copy-start(f32[31,96]{1,0:T(8,128)} %param.18) | copy-start | bytes 35716
  85.8 22.1 %collective-permute-start = (bf16[30,96]{0,1:T(8,128)(2,1)S(1)}, bf16[30,96]{0,1:T(8,128)(2,1)S(1)}, u32[]{:S(2)}, u32[]{:S(2)}) collective-permute-start(bf16[30,96]{0,1:T(8,128)(2,1)S(1)} %slice.276), channel_id=1, source_target_pairs={{0,16},{16,32},{32,48},{48,64},{64,80},{80,96},{96,112},{112,128},... | collective-permute-start | bytes 17288 | tf_op jit(solution)/shard_map/ppermute | solution.py:26
  90.9 36.5 %copy-start.10 = (bf16[1024,128]{1,0:T(8,128)(2,1)S(1)}, bf16[1024,128]{1,0:T(8,128)(2,1)}, u32[]{:S(2)}) copy-start(bf16[1024,128]{1,0:T(8,128)(2,1)} %get-tuple-element.5) | copy-start | bytes 786436
  127.4 1.0 copy-start.9
  127.8 3.0 %slice-start = ((bf16[16,104,128]{2,1,0:T(8,128)(2,1)}), bf16[16,96,128]{2,1,0:T(8,128)(2,1)S(1)}, s32[]{:S(2)}) async-start(bf16[16,104,128]{2,1,0:T(8,128)(2,1)} %copy-done.4), calls=%async_computation.3 | async-start | bytes 786432 | tf_op jit(solution)/shard_map/slice | solution.py:90
  128.7 3.1 %collective-permute-start.7 = (bf16[2,32,512]{2,1,0:T(8,128)(2,1)S(1)}, bf16[2,32,512]{2,1,0:T(8,128)(2,1)S(1)}, u32[]{:S(2)}, u32[]{:S(2)}) collective-permute-start(bf16[2,32,512]{2,1,0:T(8,128)(2,1)S(1)} %fusion.27), channel_id=1, source_target_pairs={{0,1},{1,0},{2,3},{3,2},{4,5},{5,4},{6,7},{7,6},{8,9},{9,8},{10,11... | collective-permute-start | bytes 196616 | tf_op jit(solution)/shard_map/ppermute | solution.py:30
  131.9 21.6 %collective-permute-start.8 = (bf16[32,512]{1,0:T(8,128)(2,1)S(1)}, bf16[32,512]{1,0:T(8,128)(2,1)S(1)}, u32[]{:S(2)}, u32[]{:S(2)}) collective-permute-start(bf16[32,512]{1,0:T(8,128)(2,1)S(1)} %fusion.29), channel_id=1, source_target_pairs={{0,2},{2,0},{1,3},{3,1},{4,6},{6,4},{5,7},{7,5},{8,10},{10,8},{9,1... | collective-permute-start | bytes 98312 | tf_op jit(solution)/shard_map/ppermute | solution.py:30
